TPU v7x, 256 devices: a whole 4x4x8 slice. The times are simulated.
256 devices in a mesh: ep: 16 (over y, x), tp: 16 (over z, core).
Axes of the slice: x: 4, y: 4, z: 8, core: 2. Of those that a mesh axis runs over, the one named last changes fastest.
Arguments:
- residual: bfloat16 [512, 2048], P('ep'), may hold values from -6 to 6
- mixer_gain: float32 [2048], replicated, may hold values from 0.1 to 1.9
- gate_proj: bfloat16 [2048, 2048], P('ep', 'tp'), may hold values from -0.125 to 0.125
- input_proj: bfloat16 [2048, 2048], P('ep', 'tp'), may hold values from -0.125 to 0.125
- write_proj: bfloat16 [2048, 2048], P('ep', 'tp'), may hold values from -0.125 to 0.125
- read_proj: bfloat16 [2048, 2048], P('ep', 'tp'), may hold values from -0.125 to 0.125
- step_proj: bfloat16 [2048, 32], replicated, may hold values from -0.125 to 0.125
- conv_weight: float32 [4, 3, 2048], replicated, may hold values from -3 to 3
- step_bias: float32 [32], replicated, may hold values from -4 to 0
- log_rate: float32 [32], replicated, may hold values from 0 to 2.5
- skip_gain: float32 [32], replicated, may hold values from -4 to 4
- group_gain: float32 [2048], replicated, may hold values from 0.1 to 1.9
- ssm_state: float32 [512, 32, 64, 128], P('ep', 'tp'), may hold values from -2 to 2
- conv_state: bfloat16 [512, 3, 3, 2048], P('ep', None, None, 'tp'), may hold values from -6 to 6
- out_proj: bfloat16 [2048, 2048], P('tp'), may hold values from -0.125 to 0.125
- ffn_gain: float32 [2048], replicated, may hold values from 0.1 to 1.9
- routes: int32 [512, 2], P('ep'), may hold values from 0 to 31, all different within a row; in each aligned block of 32 rows (0 to 31, 32 to 63, ...) at most 4 rows name the same one
- route_weight: float32 [512, 2], P('ep'), may hold values from 0.2 to 1
- expert_gate: bfloat16 [32, 2048, 2048], P('ep', None, 'tp'), may hold values from -0.125 to 0.125
- expert_up: bfloat16 [32, 2048, 2048], P('ep', None, 'tp'), may hold values from -0.125 to 0.125
- expert_down: bfloat16 [32, 2048, 2048], P('ep', 'tp'), may hold values from -0.125 to 0.125
- dense_gate: bfloat16 [2048, 2048], P(None, 'tp'), may hold values from -0.125 to 0.125
- dense_up: bfloat16 [2048, 2048], P(None, 'tp'), may hold values from -0.125 to 0.125
- dense_down: bfloat16 [2048, 2048], P('tp'), may hold values from -0.125 to 0.125
- blend_weight: bfloat16 [2048], replicated, may hold values from -0.125 to 0.125
Outputs:
- layer_out: bfloat16 [512, 2048], P('ep', 'tp')
- new_state: float32 [512, 32, 64, 128], P('ep', 'tp')
- new_conv: bfloat16 [512, 3, 3, 2048], P('ep', None, None, 'tp')
Inputs may be any that keep to these rules, and one draw needn't show every extreme that they name: `routes`: each row names 2 different experts. Within the 32 rows of one index of ep no expert is named by more than 4 rows, and in some such block some expert is named by exactly 4 rows.
All inputs are finite; a program needn't handle non-finite values.
Results may differ from a plain program's by a relative error of at most 0.015.
Values may be sent and summed in bfloat16 or wider, within the bound.
A program may use at most 128 MiB of HBM per device.

v0:
```python
import jax
import jax.numpy as jnp
from jax import lax
from jax.sharding import PartitionSpec as P

epsilon = 1e-06


def in_blocks(array, dim, count):
    before, after = (array.shape[:dim], array.shape[dim + 1 :])
    return jnp.moveaxis(array.reshape(*before, count, -1, *after), dim, 0)


def sum_at_owner(array, axis, dim):
    parts = in_blocks(array, dim, lax.axis_size(axis))
    arrived = lax.all_to_all(parts, axis, split_axis=0, concat_axis=0, tiled=True)
    return arrived.sum(axis=0)


def filled_up(lines, count):
    spare = -lines.shape[0] % count
    if not spare:
        return lines
    return jnp.concatenate([lines, jnp.zeros((spare, *lines.shape[1:]), lines.dtype)])


def joined_along(parts, dim):
    shape = list(parts.shape[1:])
    shape[dim] *= parts.shape[0]
    return jnp.moveaxis(parts, 0, dim).reshape(shape)


def sent_to_all(array, axis):
    copies = jnp.broadcast_to(array, (lax.axis_size(axis), *array.shape))
    return lax.all_to_all(copies, axis, split_axis=0, concat_axis=0, tiled=True)


def gather_directly(array, axis, dim):
    return joined_along(sent_to_all(array, axis), dim)


def nested_sum(array, axes):
    lines = array.reshape(-1, array.shape[-1])
    padded = filled_up(lines, lax.axis_size(axes))
    whole = gather_directly(sum_at_owner(padded, axes, 0), axes, 0)
    return lax.slice_in_dim(whole, 0, len(lines)).reshape(array.shape)


def sum_at_owner_2(array, axis, dim):
    parts = in_blocks(array, dim, lax.axis_size(axis))
    arrived = lax.all_to_all(parts, axis, split_axis=0, concat_axis=0, tiled=True)
    return arrived.astype(jnp.float32).sum(axis=0)


def rms_rows(values, gain_vector):
    floats_in = values.astype(jnp.float32)
    return (
        floats_in
        * lax.rsqrt(jnp.mean(floats_in * floats_in, axis=-1, keepdims=True) + epsilon)
        * gain_vector
    )


def on_device(
    residual,
    mixer_gain,
    gate_proj,
    input_proj,
    write_proj,
    read_proj,
    step_proj,
    conv_weight,
    step_bias,
    log_rate,
    skip_gain,
    group_gain,
    ssm_state,
    conv_state,
    out_proj,
    ffn_gain,
    routes,
    route_weight,
    expert_gate,
    expert_up,
    expert_down,
    dense_gate,
    dense_up,
    dense_down,
    blend_weight,
):
    seq_rows = residual.shape[0]
    col_width = gate_proj.shape[1]
    heads_here = ssm_state.shape[1]
    head_dim = ssm_state.shape[2]
    state_dim = ssm_state.shape[3]
    groups_here = col_width // state_dim
    tp_rank = lax.axis_index("tp")
    head_start = tp_rank * heads_here
    chan_start = tp_rank * col_width
    normed = rms_rows(residual, mixer_gain).astype(jnp.bfloat16)
    joined = jnp.concatenate((gate_proj, input_proj, write_proj, read_proj), axis=1)
    pieces = lax.all_to_all(normed, "ep", split_axis=1, concat_axis=0, tiled=True)
    summed = sum_at_owner(jnp.dot(pieces, joined, preferred_element_type=jnp.float32), "ep", 0)
    projected = summed.astype(jnp.bfloat16)
    z_proj = projected[:, :col_width]
    x_proj = projected[:, col_width : 2 * col_width]
    b_proj = projected[:, 2 * col_width : 3 * col_width]
    c_proj = projected[:, 3 * col_width :]
    step_cols = lax.dynamic_slice_in_dim(step_proj, head_start, heads_here, 1)
    step_raw = jnp.dot(normed, step_cols, preferred_element_type=jnp.float32)
    newest = jnp.stack((x_proj, b_proj, c_proj), axis=1)[:, None]
    stacked = jnp.concatenate((conv_state, newest), axis=1)
    new_conv = stacked[:, 1:]
    conv_taps = lax.dynamic_slice_in_dim(conv_weight, chan_start, col_width, 2)
    activated = jax.nn.silu(jnp.einsum("skcw,kcw->scw", stacked.astype(jnp.float32), conv_taps))
    per_group = heads_here // groups_here
    x_act = activated[:, 0].reshape(seq_rows, heads_here, head_dim)
    b_act = jnp.repeat(activated[:, 1].reshape(seq_rows, groups_here, state_dim), per_group, axis=1)
    c_act = jnp.repeat(activated[:, 2].reshape(seq_rows, groups_here, state_dim), per_group, axis=1)
    step_size = jax.nn.softplus(
        step_raw + lax.dynamic_slice_in_dim(step_bias, head_start, heads_here, 0)
    )
    decay_rate = jnp.exp(lax.dynamic_slice_in_dim(log_rate, head_start, heads_here, 0))
    decay_factor = jnp.exp(-decay_rate * step_size)
    new_state = (
        decay_factor[:, :, None, None] * ssm_state
        + (step_size[:, :, None] * x_act)[..., None] * b_act[:, :, None, :]
    )
    skip_here = lax.dynamic_slice_in_dim(skip_gain, head_start, heads_here, 0)
    ssm_out = jnp.einsum("shpn,shn->shp", new_state, c_act) + skip_here[None, :, None] * x_act
    gated_out = ssm_out.reshape(seq_rows, col_width) * jax.nn.silu(z_proj.astype(jnp.float32))
    grouped = gated_out.reshape(seq_rows, groups_here, col_width // groups_here)
    grouped = grouped * lax.rsqrt(jnp.mean(grouped * grouped, axis=-1, keepdims=True) + epsilon)
    gain_here = lax.dynamic_slice_in_dim(group_gain, chan_start, col_width, 0)
    mixed_out = (grouped.reshape(seq_rows, col_width) * gain_here).astype(jnp.bfloat16)
    mixer_total = nested_sum(jnp.dot(mixed_out, out_proj, preferred_element_type=jnp.float32), "tp")
    resid_mid = (residual.astype(jnp.float32) + mixer_total).astype(jnp.bfloat16)
    normed_ffn = rms_rows(resid_mid, ffn_gain).astype(jnp.bfloat16)
    top_count = routes.shape[1]
    experts_here = expert_gate.shape[0]
    ep_count = lax.axis_size("ep")
    model_width = normed_ffn.shape[1]
    total_experts = experts_here * ep_count
    capacity = max(2, 2 * seq_rows * top_count // total_experts)
    flat_routes = routes.reshape(-1)
    onehot = (flat_routes[:, None] == jnp.arange(total_experts, dtype=jnp.int32)[None, :]).astype(
        jnp.int32
    )
    slot_rank = jnp.sum((jnp.cumsum(onehot, axis=0) - onehot) * onehot, axis=1)
    position = flat_routes * capacity + slot_rank
    placing = (
        jnp.arange(total_experts * capacity, dtype=jnp.int32)[:, None] == position[None, :]
    ).astype(jnp.bfloat16)
    outgoing = jnp.dot(
        placing, jnp.repeat(normed_ffn, top_count, axis=0), preferred_element_type=jnp.float32
    ).astype(jnp.bfloat16)
    outgoing = outgoing.reshape(total_experts, 1, capacity, model_width)
    received = lax.all_to_all(outgoing, "ep", split_axis=0, concat_axis=1, tiled=True)
    item_count = received.shape[2]
    expert_rows = received.reshape(experts_here, ep_count * item_count, received.shape[3])
    gate_val = jnp.einsum(
        "erd,edf->erf", expert_rows, expert_gate, preferred_element_type=jnp.float32
    )
    up_val = jnp.einsum("erd,edf->erf", expert_rows, expert_up, preferred_element_type=jnp.float32)
    hidden = (jax.nn.silu(gate_val) * up_val).astype(jnp.bfloat16)
    partial_out = jnp.einsum(
        "erf,efd->erd", hidden, expert_down, preferred_element_type=jnp.float32
    )
    partial_out = partial_out.reshape(experts_here, ep_count, item_count, partial_out.shape[2])
    reduced = sum_at_owner_2(partial_out.astype(jnp.bfloat16), "tp", 3).astype(jnp.bfloat16)
    returned = lax.all_to_all(reduced, "ep", split_axis=1, concat_axis=0, tiled=True)
    back_rows = returned.reshape(total_experts * capacity, returned.shape[3])
    picked = jnp.dot(placing.T, back_rows, preferred_element_type=jnp.float32)
    expert_mix = jnp.sum(
        picked.reshape(seq_rows, top_count, back_rows.shape[1]) * route_weight[..., None], axis=1
    )
    gate_val = jnp.dot(normed_ffn, dense_gate, preferred_element_type=jnp.float32)
    up_val = jnp.dot(normed_ffn, dense_up, preferred_element_type=jnp.float32)
    dense_hidden = (jax.nn.silu(gate_val) * up_val).astype(jnp.bfloat16)
    dense_out = sum_at_owner_2(
        jnp.dot(dense_hidden, dense_down, preferred_element_type=jnp.float32).astype(jnp.bfloat16),
        "tp",
        1,
    )
    mix_weight = jax.nn.sigmoid(
        jnp.dot(normed_ffn, blend_weight, preferred_element_type=jnp.float32)
    )
    slice_width = dense_out.shape[1]
    own_resid = lax.dynamic_slice_in_dim(resid_mid, tp_rank * slice_width, slice_width, 1).astype(
        jnp.float32
    )
    layer_out = (own_resid + expert_mix + mix_weight[:, None] * dense_out).astype(jnp.bfloat16)
    return (layer_out, new_state, new_conv)


def solution(mesh):
    return jax.shard_map(
        on_device,
        mesh=mesh,
        in_specs=(
            P("ep", None),
            P(),
            P("ep", "tp"),
            P("ep", "tp"),
            P("ep", "tp"),
            P("ep", "tp"),
            P(),
            P(),
            P(),
            P(),
            P(),
            P(),
            P("ep", "tp", None, None),
            P("ep", None, None, "tp"),
            P("tp", None),
            P(),
            P("ep", None),
            P("ep", None),
            P("ep", None, "tp"),
            P("ep", None, "tp"),
            P("ep", "tp", None),
            P(None, "tp"),
            P(None, "tp"),
            P("tp", None),
            P(),
        ),
        out_specs=(P("ep", "tp"), P("ep", "tp", None, None), P("ep", None, None, "tp")),
        check_vma=False,
    )
```

profile of v0, /device:TPU:1, one launch (start us, length us, event | category | flops | bytes accessed | tf_op | source)
XLA Modules:
  0.0 146.4 jit_solution(9800369784747976771)
XLA Ops:
  0.7 1.1 fusion.13
  1.8 1.0 copy_bitcast_fusion.2
  2.9 14.2 %all_to_all.71 = bf16[32,16,128]{2,0,1:T(8,128)(2,1)S(1)} all-to-all(bf16[32,16,128]{2,0,1:T(8,128)(2,1)S(1)} %copy_bitcast_fusion.2), channel_id=1, replica_groups=mesh['ep'=16,'tp'=16] {'ep'}, dimensions={1} | all-to-all | bytes 262144 | tf_op jit(solution)/shard_map/all_to_all | solution.py:102
  17.1 2.1 %fusion.17 = f32[16,32,512]{2,1,0:T(8,128)} fusion(bf16[128,128]{1,0:T(8,128)(2,1)} %param.30, bf16[128,128]{1,0:T(8,128)(2,1)} %param.29, bf16[128,128]{1,0:T(8,128)(2,1)} %param.28, bf16[128,128]{1,0:T(8,128)(2,1)} %param.27, bf16[32,16,128]{2,0,1:T(8,128)(2,1)S(1)} %all_to_all.71), kind=kOutput, calls=%fused_computation.38 | convolution fusion | flops 67633152 | bytes 1310720 | tf_op jit(solution)/shard_map/dot_general | solution.py:103
  19.2 3.8 %all-to-all-start.1 = ((f32[16,32,512]{2,1,0:T(8,128)}), f32[16,32,512]{2,1,0:T(8,128)S(1)}, u32[]{:S(2)}, u32[]{:S(2)}) async-start(f32[16,32,512]{2,1,0:T(8,128)} %fusion.17), calls=%async_computation.1 | async-start | bytes 2097152 | tf_op jit(solution)/shard_map/all_to_all | solution.py:16
  24.7 1.0 multiply_exponential_fusion
  25.9 12.1 %all-to-all-done.1 = f32[16,32,512]{2,1,0:T(8,128)S(1)} async-done(((f32[16,32,512]{2,1,0:T(8,128)}), f32[16,32,512]{2,1,0:T(8,128)S(1)}, u32[]{:S(2)}, u32[]{:S(2)}) %all-to-all-start.1) | async-done | bytes 1048608 | tf_op jit(solution)/shard_map/all_to_all | solution.py:16
  38.9 2.0 %multiply_add_fusion = f32[32,2,64,128]{3,2,1,0:T(8,128)S(1)} fusion(f32[32,2,64,128]{3,2,1,0:T(8,128)} %param.37, f32[32,128]{1,0:T(8,128)S(1)} %get-tuple-element.6, f32[32,2,64]{2,1,0:T(2,128)S(1)} %broadcast_multiply_fusion, f32[32,2]{1,0:T(8,128)S(1)} %copy.53), kind=kLoop, calls=%fused_computation.3 | loop fusion | flops 1572864 | bytes 4227328 | tf_op jit(solution)/shard_map/add | solution.py:126
  42.0 1.2 fusion.8
  43.3 0.9 copy.57
  44.2 11.8 %all-to-all-start.2 = ((f32[16,2,2048]{2,1,0:T(2,128)}), f32[16,2,2048]{2,1,0:T(2,128)S(1)}, u32[]{:S(2)}, u32[]{:S(2)}) async-start(f32[16,2,2048]{2,1,0:T(2,128)} %copy.57), calls=%async_computation.2 | async-start | bytes 524288 | tf_op jit(solution)/shard_map/all_to_all | solution.py:16
  56.2 11.4 %all-to-all-done.2 = f32[16,2,2048]{2,1,0:T(2,128)S(1)} async-done(((f32[16,2,2048]{2,1,0:T(2,128)}), f32[16,2,2048]{2,1,0:T(2,128)S(1)}, u32[]{:S(2)}, u32[]{:S(2)}) %all-to-all-start.2) | async-done | bytes 262176 | tf_op jit(solution)/shard_map/all_to_all | solution.py:16
  67.7 0.8 broadcast_in_dim.7
  68.5 3.4 %all-to-all-start.3 = ((f32[16,2,2048]{2,1,0:T(2,128)}), f32[16,2,2048]{2,1,0:T(2,128)S(1)}, u32[]{:S(2)}, u32[]{:S(2)}) async-start(f32[16,2,2048]{2,1,0:T(2,128)} %broadcast_in_dim.7), calls=%async_computation.3 | async-start | bytes 524288 | tf_op jit(solution)/shard_map/all_to_all | solution.py:35
  72.3 10.8 %all-to-all-done.3 = f32[16,2,2048]{2,1,0:T(2,128)S(1)} async-done(((f32[16,2,2048]{2,1,0:T(2,128)}), f32[16,2,2048]{2,1,0:T(2,128)S(1)}, u32[]{:S(2)}, u32[]{:S(2)}) %all-to-all-start.3) | async-done | bytes 262176 | tf_op jit(solution)/shard_map/all_to_all | solution.py:35
  84.2 13.8 %all_to_all.72 = bf16[32,1,4,2048]{3,2,1,0:T(4,128)(2,1)S(1)} all-to-all(bf16[32,1,4,2048]{3,2,1,0:T(4,128)(2,1)S(1)} %bitcast.105), channel_id=1, replica_groups=mesh['ep'=16,'tp'=16] {'ep'}, dimensions={0} | all-to-all | bytes 1048576 | tf_op jit(solution)/shard_map/all_to_all | solution.py:158
  98.5 1.5 %fusion.65 = f32[2,64,128]{2,1,0:T(8,128)S(1)} fusion(bf16[2,64,2048]{2,1,0:T(8,128)(2,1)S(1)} %reshape.148, bf16[2,2048,128]{2,1,0:T(8,128)(2,1)} %param.43), kind=kOutput, calls=%fused_computation.110 | convolution fusion | flops 67108864 | bytes 1638400 | tf_op jit(solution)/shard_map/erd,edf->erf/dot_general | solution.py:161
  100.8 1.1 copy.91
  101.8 4.7 %all-to-all-start.5 = ((bf16[16,2,16,4,128]{4,3,2,1,0:T(4,128)(2,1)}), bf16[16,2,16,4,128]{4,3,2,1,0:T(4,128)(2,1)S(1)}, u32[]{:S(2)}, u32[]{:S(2)}) async-start(bf16[16,2,16,4,128]{4,3,2,1,0:T(4,128)(2,1)} %bitcast.100), calls=%async_computation.5 | async-start | bytes 1048576 | tf_op jit(solution)/shard_map/all_to_all | solution.py:51
  108.0 15.9 %all-to-all-done.5 = bf16[16,2,16,4,128]{4,3,2,1,0:T(4,128)(2,1)S(1)} async-done(((bf16[16,2,16,4,128]{4,3,2,1,0:T(4,128)(2,1)}), bf16[16,2,16,4,128]{4,3,2,1,0:T(4,128)(2,1)S(1)}, u32[]{:S(2)}, u32[]{:S(2)}) %all-to-all-start.5) | async-done | bytes 524320 | tf_op jit(solution)/shard_map/all_to_all | solution.py:51
  123.9 3.4 %all-to-all-start.7 = ((bf16[16,32,128]{2,1,0:T(8,128)(2,1)}), bf16[16,32,128]{2,1,0:T(8,128)(2,1)S(1)}, u32[]{:S(2)}, u32[]{:S(2)}) async-start(bf16[16,32,128]{2,1,0:T(8,128)(2,1)} %bitcast.103), calls=%async_computation.7 | async-start | bytes 262144 | tf_op jit(solution)/shard_map/all_to_all | solution.py:51
  129.0 6.7 %all-to-all-done.7 = bf16[16,32,128]{2,1,0:T(8,128)(2,1)S(1)} async-done(((bf16[16,32,128]{2,1,0:T(8,128)(2,1)}), bf16[16,32,128]{2,1,0:T(8,128)(2,1)S(1)}, u32[]{:S(2)}, u32[]{:S(2)}) %all-to-all-start.7) | async-done | bytes 131104 | tf_op jit(solution)/shard_map/all_to_all | solution.py:51
  135.7 3.5 %all-to-all-start.6 = ((bf16[2,16,4,128]{3,2,0,1:T(4,128)(2,1)}), bf16[2,16,4,128]{3,2,0,1:T(4,128)(2,1)S(1)}, u32[]{:S(2)}, u32[]{:S(2)}) async-start(bf16[2,16,4,128]{3,2,0,1:T(4,128)(2,1)} %copy.63), calls=%async_computation.6 | async-start | bytes 65536 | tf_op jit(solution)/shard_map/all_to_all | solution.py:171
  139.2 6.4 %all-to-all-done.6 = bf16[2,16,4,128]{3,2,0,1:T(4,128)(2,1)S(1)} async-done(((bf16[2,16,4,128]{3,2,0,1:T(4,128)(2,1)}), bf16[2,16,4,128]{3,2,0,1:T(4,128)(2,1)S(1)}, u32[]{:S(2)}, u32[]{:S(2)}) %all-to-all-start.6) | async-done | bytes 32800 | tf_op jit(solution)/shard_map/all_to_all | solution.py:171
  (94 shorter events, 10.5 us)
Async XLA Ops:
  0.6 99.4 %copy-start = (bf16[2,128,2048]{2,1,0:T(8,128)(2,1)S(1)}, bf16[2,128,2048]{2,1,0:T(8,128)(2,1)}, u32[]{:S(2)}) copy-start(bf16[2,128,2048]{2,1,0:T(8,128)(2,1)} %param.45) | copy-start | bytes 3145732
  0.6 24.0 %copy-start.2 = (bf16[32,2048]{1,0:T(8,128)(2,1)S(1)}, bf16[32,2048]{1,0:T(8,128)(2,1)}, u32[]{:S(2)}) copy-start(bf16[32,2048]{1,0:T(8,128)(2,1)} %param.25) | copy-start | bytes 393220
  0.7 24.0 %copy-start.11 = (f32[2048]{0:T(1024)S(1)}, f32[2048]{0:T(1024)}, u32[]{:S(2)}) copy-start(f32[2048]{0:T(1024)} %param.26) | copy-start | bytes 24580
  0.7 22.3 %copy-start.16 = (f32[32]{0:T(128)S(1)}, f32[32]{0:T(128)}, u32[]{:S(2)}) copy-start(f32[32]{0:T(128)} %param.33) | copy-start | bytes 388
  0.7 22.4 %copy-start.17 = (f32[32]{0:T(128)S(1)}, f32[32]{0:T(128)}, u32[]{:S(2)}) copy-start(f32[32]{0:T(128)} %param.35) | copy-start | bytes 388
  0.7 23.9 %copy-start.18 = (f32[32]{0:T(128)S(1)}, f32[32]{0:T(128)}, u32[]{:S(2)}) copy-start(f32[32]{0:T(128)} %param.34) | copy-start | bytes 388
  19.2 18.9 %copy-start.7 = (bf16[32,3,3,128]{3,0,2,1:T(8,128)(2,1)S(1)}, bf16[32,3,3,128]{3,0,2,1:T(8,128)(2,1)}, u32[]{:S(2)}) copy-start(bf16[32,3,3,128]{3,0,2,1:T(8,128)(2,1)} %param.38) | copy-start | bytes 221188
  19.2 18.8 %all-to-all-start.1 = ((f32[16,32,512]{2,1,0:T(8,128)}), f32[16,32,512]{2,1,0:T(8,128)S(1)}, u32[]{:S(2)}, u32[]{:S(2)}) async-start(f32[16,32,512]{2,1,0:T(8,128)} %fusion.17), calls=%async_computation.1 | async-start | bytes 2097152 | tf_op jit(solution)/shard_map/all_to_all | solution.py:16
  40.9 3.2 %copy-start.1 = (f32[32,2,64,128]{3,2,1,0:T(8,128)}, f32[32,2,64,128]{3,2,1,0:T(8,128)S(1)}, u32[]{:S(2)}) copy-start(f32[32,2,64,128]{3,2,1,0:T(8,128)S(1)} %multiply_add_fusion) | copy-start | bytes 6291460
  41.0 15.0 %copy-start.14 = (s32[32,2]{0,1:T(2,128)S(1)}, s32[32,2]{0,1:T(2,128)}, u32[]{:S(2)}) copy-start(s32[32,2]{0,1:T(2,128)} %param.41) | copy-start | bytes 772
  42.0 41.4 %copy-start.12 = (f32[2048]{0:T(1024)S(1)}, f32[2048]{0:T(1024)}, u32[]{:S(2)}) copy-start(f32[2048]{0:T(1024)} %param.40) | copy-start | bytes 24580
  44.2 23.4 %all-to-all-start.2 = ((f32[16,2,2048]{2,1,0:T(2,128)}), f32[16,2,2048]{2,1,0:T(2,128)S(1)}, u32[]{:S(2)}, u32[]{:S(2)}) async-start(f32[16,2,2048]{2,1,0:T(2,128)} %copy.57), calls=%async_computation.2 | async-start | bytes 524288 | tf_op jit(solution)/shard_map/all_to_all | solution.py:16
  68.5 14.6 %all-to-all-start.3 = ((f32[16,2,2048]{2,1,0:T(2,128)}), f32[16,2,2048]{2,1,0:T(2,128)S(1)}, u32[]{:S(2)}, u32[]{:S(2)}) async-start(f32[16,2,2048]{2,1,0:T(2,128)} %broadcast_in_dim.7), calls=%async_computation.3 | async-start | bytes 524288 | tf_op jit(solution)/shard_map/all_to_all | solution.py:35
  98.1 1.9 %copy-start.3 = (bf16[2,2048,128]{2,1,0:T(8,128)(2,1)S(1)}, bf16[2,2048,128]{2,1,0:T(8,128)(2,1)}, u32[]{:S(2)}) copy-start(bf16[2,2048,128]{2,1,0:T(8,128)(2,1)} %param.44) | copy-start | bytes 3145732
  100.6 6.0 %copy-start.13 = (bf16[2048]{0:T(1024)(128)(2,1)S(1)}, bf16[2048]{0:T(1024)(128)(2,1)}, u32[]{:S(2)}) copy-start(bf16[2048]{0:T(1024)(128)(2,1)} %param.49) | copy-start | bytes 12292
  100.6 6.1 %copy-start.4 = (bf16[2048,128]{1,0:T(8,128)(2,1)S(1)}, bf16[2048,128]{1,0:T(8,128)(2,1)}, u32[]{:S(2)}) copy-start(bf16[2048,128]{1,0:T(8,128)(2,1)} %param.46) | copy-start | bytes 1572868
  100.6 6.3 %copy-start.5 = (bf16[128,2048]{1,0:T(8,128)(2,1)S(1)}, bf16[128,2048]{1,0:T(8,128)(2,1)}, u32[]{:S(2)}) copy-start(bf16[128,2048]{1,0:T(8,128)(2,1)} %param.48) | copy-start | bytes 1572868
  100.7 6.2 %copy-start.6 = (bf16[2048,128]{1,0:T(8,128)(2,1)S(1)}, bf16[2048,128]{1,0:T(8,128)(2,1)}, u32[]{:S(2)}) copy-start(bf16[2048,128]{1,0:T(8,128)(2,1)} %param.47) | copy-start | bytes 1572868
  100.7 26.6 %copy-start.8 = (bf16[32,3,3,128]{3,0,2,1:T(8,128)(2,1)S(1)}, bf16[32,3,3,128]{3,0,2,1:T(8,128)(2,1)}, u32[]{:S(2)}) copy-start(bf16[32,3,3,128]{3,0,2,1:T(8,128)(2,1)} %param.38) | copy-start | bytes 221188
  100.7 26.5 %copy-start.10 = (bf16[32,1,3,128]{3,0,2,1:T(8,128)(2,1)S(1)}, bf16[32,1,3,128]{3,0,2,1:T(8,128)(2,1)}, u32[]{:S(2)}) copy-start(bf16[32,1,3,128]{3,0,2,1:T(8,128)(2,1)} %copy-done.9) | copy-start | bytes 73732
  101.8 22.0 %all-to-all-start.5 = ((bf16[16,2,16,4,128]{4,3,2,1,0:T(4,128)(2,1)}), bf16[16,2,16,4,128]{4,3,2,1,0:T(4,128)(2,1)S(1)}, u32[]{:S(2)}, u32[]{:S(2)}) async-start(bf16[16,2,16,4,128]{4,3,2,1,0:T(4,128)(2,1)} %bitcast.100), calls=%async_computation.5 | async-start | bytes 1048576 | tf_op jit(solution)/shard_map/all_to_all | solution.py:51
  106.6 39.0 %copy-start.15 = (f32[32,2]{0,1:T(2,128)S(1)}, f32[32,2]{0,1:T(2,128)}, u32[]{:S(2)}) copy-start(f32[32,2]{0,1:T(2,128)} %param.42) | copy-start | bytes 772
  123.9 11.8 %all-to-all-start.7 = ((bf16[16,32,128]{2,1,0:T(8,128)(2,1)}), bf16[16,32,128]{2,1,0:T(8,128)(2,1)S(1)}, u32[]{:S(2)}, u32[]{:S(2)}) async-start(bf16[16,32,128]{2,1,0:T(8,128)(2,1)} %bitcast.103), calls=%async_computation.7 | async-start | bytes 262144 | tf_op jit(solution)/shard_map/all_to_all | solution.py:51
  135.7 9.9 %all-to-all-start.6 = ((bf16[2,16,4,128]{3,2,0,1:T(4,128)(2,1)}), bf16[2,16,4,128]{3,2,0,1:T(4,128)(2,1)S(1)}, u32[]{:S(2)}, u32[]{:S(2)}) async-start(bf16[2,16,4,128]{3,2,0,1:T(4,128)(2,1)} %copy.63), calls=%async_computation.6 | async-start | bytes 65536 | tf_op jit(solution)/shard_map/all_to_all | solution.py:171
  (1 other events, 0.6 us)
where the time goes:
time: 147 us; the launch traced here: 146 us
  waiting for transfers between devices  63.2 us (43%)
  starting transfers between devices  30.6 us (21%)
  blocking collectives  28.1 us (19%)
  matrix products  8.09 us (6%)
  local copies, waits for them, and re-layouts  7.97 us (5%)
  other arithmetic  7.2 us (5%)
    all_to_all x2, waiting for transfers between devices, sum_at_owner(): lax.all_to_all(parts, axis, split_axis=0, concat_axis=0, tiled=True)  23.5 us
    all_to_all x2, waiting for transfers between devices, sum_at_owner_2(): lax.all_to_all(parts, axis, split_axis=0, concat_axis=0, tiled=True)  22.6 us
    all_to_all x2, starting transfers between devices, sum_at_owner(): lax.all_to_all(parts, axis, split_axis=0, concat_axis=0, tiled=True)  15.6 us
    all_to_all x1, blocking collectives, on_device(): lax.all_to_all(normed, 'ep', split_axis=1, concat_axis=0, tiled=True)  14.2 us
    all_to_all x1, blocking collectives, on_device(): lax.all_to_all(outgoing, 'ep', split_axis=0, concat_axis=1, tiled=True)  13.8 us
    all_to_all x1, waiting for transfers between devices, sent_to_all(): return lax.all_to_all(copies, axis, split_axis=0, concat_axis=0, tiled=True)  10.8 us
    all_to_all x2, starting transfers between devices, sum_at_owner_2(): lax.all_to_all(parts, axis, split_axis=0, concat_axis=0, tiled=True)  8.13 us
    all_to_all x1, waiting for transfers between devices, on_device(): lax.all_to_all(reduced, 'ep', split_axis=1, concat_axis=0, tiled=True)  6.36 us
  transfers between devices with their start and end apart: 6, of which 6 were waited for; matrix products, arithmetic and copies ran while one was open for 4% of the time, Pallas kernels for 0%

commit v1 on v0

v1 whole, which is shorter than its diff:
```python
import functools

import jax
import jax.numpy as jnp
from jax import lax
from jax.experimental import pallas as pl
from jax.experimental.pallas import tpu as pltpu
from jax.sharding import PartitionSpec as P

MESH = pl.DeviceIdType.MESH
F32 = jnp.float32
BF16 = jnp.bfloat16
EPS = 1e-06
ANY = pl.BlockSpec(memory_space=pl.ANY)
SMEM = pl.BlockSpec(memory_space=pltpu.SMEM)


def dot(a, b, dims=(((1,), (0,)), ((), ()))):
    return lax.dot_general(a, b, dims, preferred_element_type=F32)


def silu(v):
    return v * jax.nn.sigmoid(v)


def lanes(t):
    return slice(t * 128, (t + 1) * 128)


def kernel(
    residual,
    mixer_gain,
    gate_proj,
    input_proj,
    write_proj,
    read_proj,
    step_proj,
    conv_weight,
    step_bias,
    log_rate,
    skip_gain,
    group_gain,
    ssm_state,
    conv_state,
    out_proj,
    ffn_gain,
    routes,
    route_weight,
    expert_gate,
    expert_up,
    expert_down,
    dense_gate,
    dense_up,
    dense_down,
    blend_weight,
    layer_out,
    new_state,
    newest,
    res,
    mgain,
    ggain,
    fgain,
    blend,
    cw,
    sproj,
    rts,
    rw,
    cst,
    st,
    wp,
    wq,
    op,
    gu,
    dn,
    dgu,
    ddn,
    nat,
    np_,
    nq,
    rp,
    rq,
    sp,
    sq,
    r2p,
    r2q,
    dec,
    dxs,
    bs,
    cs,
    ys,
    nw,
    mixer_half,
    mixer_own,
    mixer_pair,
    rs_out,
    rs_in,
    rm,
    rmf_own,
    place,
    outb,
    rx,
    xn,
    half_e,
    own_e,
    pair_e,
    ret,
    back,
    xd,
    half_d,
    own_d,
    pair_d,
    rs2_out,
    rs2_in,
    lout,
    load_sem,
    store_sem,
    s1,
    r1,
    s2,
    r2,
    sz,
    rz,
    spair,
    rpair,
    sg,
    rg,
    sf,
    rf,
    sr,
    rr,
):
    E = lax.axis_index("ep")
    T = lax.axis_index("tp")
    Y, X = lax.div(E, 4), lax.rem(E, 4)
    Z, C = lax.div(T, 2), lax.rem(T, 2)
    pair = Z * 2 + (1 - C)

    def ep_at(d):
        dy, dx = lax.div(d, 4), lax.rem(d, 4)
        return lax.rem(Y + dy, 4) * 4 + lax.rem(X + dx, 4)

    def ep_from(d):
        dy, dx = lax.div(d, 4), lax.rem(d, 4)
        return lax.rem(Y + 4 - dy, 4) * 4 + lax.rem(X + 4 - dx, 4)

    def tp_at(d):
        return lax.rem(Z + d, 8) * 2 + C

    def loop(lo, hi, fn):
        lax.fori_loop(lo, hi, lambda i, c: (fn(i), c)[1], 0)

    def send(src, dst, ssem, rsem, ep, tp):
        return pltpu.make_async_remote_copy(
            src_ref=src,
            dst_ref=dst,
            send_sem=ssem,
            recv_sem=rsem,
            device_id={"ep": ep, "tp": tp},
            device_id_type=MESH,
        )

    bar = pltpu.get_barrier_semaphore()
    loop(
        1,
        16,
        lambda d: pl.semaphore_signal(
            bar, inc=1, device_id={"ep": ep_at(d), "tp": T}, device_id_type=MESH
        ),
    )
    loop(
        1,
        8,
        lambda d: pl.semaphore_signal(
            bar, inc=1, device_id={"ep": E, "tp": tp_at(d)}, device_id_type=MESH
        ),
    )
    pl.semaphore_signal(bar, inc=1, device_id={"ep": E, "tp": pair}, device_id_type=MESH)

    chan = pl.ds(pl.multiple_of(T * 128, 128), 128)
    loads = {}

    def load(name, *pairs):
        first = sum(len(v) for v in loads.values())
        copies = [
            pltpu.make_async_copy(s, d, load_sem.at[first + i]) for i, (s, d) in enumerate(pairs)
        ]
        for c in copies:
            c.start()
        loads[name] = copies

    def loaded(*names):
        for name in names:
            for c in loads[name]:
                c.wait()

    load("res", (residual, res), (mixer_gain, mgain))
    load(
        "proj",
        (gate_proj, wp.at[X, :, pl.ds(0, 128)]),
        (input_proj, wp.at[X, :, pl.ds(128, 128)]),
        (write_proj, wq.at[Y, :, pl.ds(0, 128)]),
        (read_proj, wq.at[Y, :, pl.ds(128, 128)]),
    )
    load(
        "small",
        (step_proj, sproj),
        (conv_weight.at[:, :, chan], cw),
        (conv_state, cst),
        (routes, rts),
        (route_weight, rw),
    )
    load("state", (ssm_state, st))
    load("op", (out_proj, op), (group_gain, ggain))
    load("ffn", (ffn_gain, fgain), (blend_weight, blend))
    load(
        "dense",
        (dense_gate, dgu.at[:, pl.ds(0, 128)]),
        (dense_up, dgu.at[:, pl.ds(128, 128)]),
        (dense_down, ddn),
    )
    load(
        "experts",
        (expert_gate, gu.at[:, :, pl.ds(0, 128)]),
        (expert_up, gu.at[:, :, pl.ds(128, 128)]),
        (expert_down, dn),
    )

    loaded("res")
    rv = res[...].astype(F32)
    scale = lax.rsqrt(jnp.mean(rv * rv, axis=-1, keepdims=True) + EPS)
    for t in range(16):
        blk = (rv[:, lanes(t)] * scale * mgain[t : t + 1, :]).astype(BF16)
        nat[:, lanes(t)] = blk
        np_[t // 4, :, lanes(t % 4)] = blk
        nq[t % 4, :, lanes(t // 4)] = blk
    rp[0] = np_[Y]
    rq[0] = nq[X]

    loaded("proj")
    pl.semaphore_wait(bar, 23)

    def y_at(d):
        return lax.rem(Y + d, 4) * 4 + X

    def x_at(d):
        return Y * 4 + lax.rem(X + d, 4)

    def w_p(d):
        return send(wp.at[X], wp.at[X], s1.at[d - 1], r1.at[d - 1], x_at(d), T)

    def w_q(d):
        return send(wq.at[Y], wq.at[Y], s1.at[d + 2], r1.at[d + 2], y_at(d), T)

    def n_p(d):
        return send(
            np_.at[lax.rem(Y + d, 4)], rp.at[d], s1.at[d + 5], r1.at[d + 5], y_at(d), T
        )

    def n_q(d):
        return send(
            nq.at[lax.rem(X + d, 4)], rq.at[d], s1.at[d + 8], r1.at[d + 8], x_at(d), T
        )

    for f in (w_p, w_q, n_p, n_q):
        loop(1, 4, lambda d, f=f: f(d).start())

    loaded("small")
    raw = dot(nat[...], sproj[...], (((1,), (1,)), ((), ())))
    lane32 = lax.broadcasted_iota(jnp.int32, (32, 32), 1)
    lane128 = lax.broadcasted_iota(jnp.int32, (32, 128), 1)
    dts = []
    for h in range(2):
        col = jnp.sum(jnp.where(lane32 == 2 * T + h, raw, 0.0), axis=1, keepdims=True)
        v = jnp.broadcast_to(col, (32, 128)) + step_bias[2 * T + h]
        dt = jnp.maximum(v, 0.0) + jnp.log1p(jnp.exp(-jnp.abs(v)))
        rate = jnp.exp(jnp.full((32, 128), log_rate[2 * T + h], F32))
        dec[h] = jnp.exp(-rate * dt)
        dts.append(dt)
    dt = jnp.where(lane128 < 64, dts[0], dts[1])
    skip = jnp.where(
        lane128 < 64,
        jnp.full((32, 128), skip_gain[2 * T], F32),
        jnp.full((32, 128), skip_gain[2 * T + 1], F32),
    )
    held = []
    for c in range(3):
        acc = cst[0, c].astype(F32) * cw[c, 0:1, :]
        for k in range(1, 3):
            acc = acc + cst[k, c].astype(F32) * cw[c, k : k + 1, :]
        held.append(acc)

    sub32 = lax.broadcasted_iota(jnp.int32, (32, 32), 0)
    hot = [(sub32 == rts[k : k + 1, :]).astype(F32) for k in range(2)]
    before = (sub32 < lane32).astype(BF16)
    prefix = dot((hot[0] + hot[1]).astype(BF16), before)
    slot = lax.broadcasted_iota(jnp.int32, (128, 32), 0)
    spots = []
    for k in range(2):
        rank = jnp.sum(hot[k] * prefix, axis=0, keepdims=True).astype(jnp.int32)
        spots.append((slot == rts[k : k + 1, :] * 4 + rank).astype(F32))
    place[0] = spots[0] + spots[1]
    place[1] = spots[0] * rw[0:1, :] + spots[1] * rw[1:2, :]

    loop(1, 4, lambda d: w_p(d).wait_recv())
    loop(1, 4, lambda d: n_p(d).wait_recv())
    part_p = dot(rp[...].reshape(128, 512), wp[...].reshape(512, 256))
    sp[...] = part_p.astype(BF16).reshape(4, 32, 256)

    def back_p(d):
        return send(
            sp.at[d], r2p.at[d - 1], s2.at[d - 1], r2.at[d - 1], y_at(4 - d), T
        )

    loop(1, 4, lambda d: back_p(d).start())
    loop(1, 4, lambda d: w_q(d).wait_recv())
    loop(1, 4, lambda d: n_q(d).wait_recv())
    part_q = dot(rq[...].reshape(128, 512), wq[...].reshape(512, 256))
    sq[...] = part_q.astype(BF16).reshape(4, 32, 256)

    def back_q(d):
        return send(
            sq.at[d], r2q.at[d - 1], s2.at[d + 2], r2.at[d + 2], x_at(4 - d), T
        )

    loop(1, 4, lambda d: back_q(d).start())
    own_p, own_q = part_p[0:32], part_q[0:32]
    loaded("state", "op")
    loop(1, 4, lambda d: back_p(d).wait_recv())
    for d in range(3):
        own_p = own_p + r2p[d].astype(F32)
    loop(1, 4, lambda d: back_q(d).wait_recv())
    for d in range(3):
        own_q = own_q + r2q[d].astype(F32)
    z_proj = own_p[:, 0:128].astype(BF16).astype(F32)
    fresh = [own_p[:, 128:256], own_q[:, 0:128], own_q[:, 128:256]]
    acts = []
    for c in range(3):
        row = fresh[c].astype(BF16)
        nw[c] = row
        acts.append(silu(held[c] + row.astype(F32) * cw[c, 3:4, :]))
    x_act = acts[0]
    dxs[...] = dt * x_act
    bs[...] = acts[1]
    cs[...] = acts[2]

    lane_y = lax.broadcasted_iota(jnp.int32, (64, 128), 1)

    def tokens(g):
        base = pl.multiple_of(g * 8, 8)
        dx_t = jnp.transpose(dxs[pl.ds(base, 8), :])
        yt = [jnp.zeros((64, 128), F32), jnp.zeros((64, 128), F32)]
        for i in range(8):
            s = base + i
            b_row = bs[pl.ds(s, 1), :]
            c_row = cs[pl.ds(s, 1), :]
            for h in range(2):
                ns = dec[h, pl.ds(s, 1), :] * st[s, h] + dx_t[h * 64 : h * 64 + 64, i : i + 1] * b_row
                st[s, h] = ns
                y = jnp.sum(ns * c_row, axis=1, keepdims=True)
                yt[h] = jnp.where(lane_y == i, y, yt[h])
        ys[pl.ds(base, 8), :] = jnp.transpose(jnp.concatenate(yt, axis=0))[0:8]

    loop(0, 4, tokens)
    keep_state = pltpu.make_async_copy(st, new_state, store_sem.at[0])
    keep_conv = pltpu.make_async_copy(nw, newest, store_sem.at[1])

    gated = (ys[...] + skip * x_act) * silu(z_proj)
    gated = gated * lax.rsqrt(jnp.mean(gated * gated, axis=-1, keepdims=True) + EPS)
    mixed = (gated * ggain[pl.ds(T, 1), :]).astype(BF16)
    part = dot(mixed, op[...])
    for t in range(16):
        mixer_half[t % 2, t // 2] = part[:, lanes(t)].astype(BF16)
        if t % 2 == 0:
            mixer_own[t // 2] = jnp.where(C == 0, part[:, lanes(t)], part[:, lanes(t + 1)])

    def to_pair(src, dst, i):
        return send(src, dst, spair.at[i], rpair.at[i], E, pair)

    swap_mixer = to_pair(mixer_half.at[1 - C], mixer_pair, 0)
    swap_mixer.start()
    keep_state.start()
    keep_conv.start()
    swap_mixer.wait_recv()
    mixer_own[...] = mixer_own[...] + mixer_pair[...].astype(F32)
    rs_out[...] = mixer_own[...].astype(BF16)

    def z_block(d):
        return lax.rem(Z + d, 8)

    def scatter(d):
        return send(
            rs_out.at[z_block(d)], rs_in.at[d - 1], sz.at[d - 1], rz.at[d - 1], E, tp_at(d)
        )

    loop(1, 8, lambda d: scatter(d).start())
    total = mixer_own[Z]
    resid_cols = res[:, chan].astype(F32)
    loop(1, 8, lambda d: scatter(d).wait_recv())
    for d in range(7):
        total = total + rs_in[d].astype(F32)
    rm[C, Z] = (resid_cols + total).astype(BF16)

    def gather(d):
        return send(
            rm.at[C, Z], rm.at[C, Z], sz.at[d + 6], rz.at[d + 6], E, tp_at(d)
        )

    def gather_in(d):
        return send(
            rm.at[C, z_block(8 - d)], rm.at[C, z_block(8 - d)], sz.at[d + 6], rz.at[d + 6], E, tp_at(d)
        )

    loop(1, 8, lambda d: gather(d).start())
    loaded("dense", "experts", "ffn")
    loop(1, 8, lambda d: gather_in(d).wait_recv())
    swap_resid = to_pair(rm.at[C], rm.at[C], 1)
    swap_resid.start()

    mine = rm[C]
    mine = jnp.concatenate([mine[z] for z in range(8)], axis=1)
    rows = dot(place[0].astype(BF16), mine).reshape(16, 8, 1024)
    outb[...] = jnp.concatenate([rows[:, :, :512], rows[:, :, 512:]], axis=1).astype(BF16)
    rx[C, 0] = outb[E]

    def dispatch(d):
        return send(outb.at[ep_at(d)], rx.at[C, d], sg.at[d - 1], rg.at[d - 1], ep_at(d), T)

    def forward(d):
        return send(rx.at[C, d], rx.at[C, d], sf.at[d], rf.at[d], E, pair)

    def forward_in(d):
        return send(rx.at[1 - C, d], rx.at[1 - C, d], sf.at[d], rf.at[d], E, pair)

    loop(1, 16, lambda d: dispatch(d).start())
    forward(0).start()

    to_pair(rm.at[1 - C], rm.at[1 - C], 1).wait_recv()
    ms = jnp.zeros((32, 1), F32)
    for t in range(16):
        v = rm[t % 2, t // 2].astype(F32)
        ms = ms + jnp.sum(v * v, axis=1, keepdims=True)
    scale = lax.rsqrt(ms * (1.0 / 2048) + EPS)
    logit = jnp.zeros((32, 128), F32)
    for t in range(16):
        v = rm[t % 2, t // 2].astype(F32)
        n = (v * scale * fgain[t : t + 1, :]).astype(BF16)
        xd[:, lanes(t)] = n
        logit = logit + n.astype(F32) * blend[t : t + 1, :].astype(F32)
    mix_weight = jax.nn.sigmoid(jnp.sum(logit, axis=1, keepdims=True))
    hid = dot(xd[...], dgu[...])
    hid = (silu(hid[:, 0:128]) * hid[:, 128:256]).astype(BF16)
    part = dot(hid, ddn[...]) * mix_weight
    for t in range(16):
        half_d[t % 2, t // 2] = part[:, lanes(t)].astype(BF16)
        if t % 2 == 0:
            own_d[t // 2] = jnp.where(C == 0, part[:, lanes(t)], part[:, lanes(t + 1)])
    swap_dense = to_pair(half_d.at[1 - C], pair_d, 2)
    swap_dense.start()

    def arrive(d):
        dispatch(d).wait_recv()
        forward(d).start()

    loop(1, 16, arrive)
    loop(0, 16, lambda d: forward_in(d).wait_recv())

    def side(c):
        v = rx[c].astype(F32).reshape(16, 2, 8, 512)
        return v[:, 0].reshape(128, 512), v[:, 1].reshape(128, 512)

    quarters = [side(0), side(1)]
    ms = jnp.zeros((128, 1), F32)
    for q in quarters:
        for v in q:
            ms = ms + jnp.sum(v * v, axis=1, keepdims=True)
    scale = lax.rsqrt(ms * (1.0 / 2048) + EPS)
    for t in range(16):
        zz = t // 2
        v = quarters[t % 2][zz // 4][:, lanes(zz % 4)]
        xn[:, lanes(t)] = (v * scale * fgain[t : t + 1, :]).astype(BF16)
    row = lax.broadcasted_iota(jnp.int32, (128, 128), 0)
    hids = []
    for j in range(2):
        hid = dot(xn[...], gu[j])
        hid = silu(hid[:, 0:128]) * hid[:, 128:256]
        mine = (row % 8 >= 4) if j else (row % 8 < 4)
        hids.append(jnp.where(mine, hid, 0.0).astype(BF16))
    part = dot(jnp.concatenate(hids, axis=1), dn[...].reshape(256, 2048))

    def folded(v):
        lo = v[0].reshape(16, 8, 512)
        hi = v[1].reshape(16, 8, 512)
        return jnp.concatenate([lo, hi], axis=1)

    for q in range(2):
        even = jnp.concatenate([part[:, lanes(2 * z)] for z in range(4 * q, 4 * q + 4)], axis=1)
        odd = jnp.concatenate([part[:, lanes(2 * z + 1)] for z in range(4 * q, 4 * q + 4)], axis=1)
        half_e[0, q] = even.astype(BF16)
        half_e[1, q] = odd.astype(BF16)
        own_e[q] = jnp.where(C == 0, even, odd)
    swap_expert = to_pair(half_e.at[1 - C], pair_e, 3)
    swap_expert.start()
    swap_expert.wait_recv()
    both = own_e[...] + pair_e[...].astype(F32)
    ret[...] = folded(both).astype(BF16)
    back[E] = ret[0]

    def give_back(d):
        return send(ret.at[d], back.at[E], sr.at[d - 1], rr.at[d - 1], ep_from(d), T)

    def give_back_in(d):
        return send(ret.at[d], back.at[ep_at(d)], sr.at[d - 1], rr.at[d - 1], ep_from(d), T)

    loop(1, 16, lambda d: give_back(d).start())
    swap_dense.wait_recv()
    own_d[...] = own_d[...] + pair_d[...].astype(F32)
    weight = place[1]
    w_hi = weight.astype(BF16)
    w_lo = (weight - w_hi.astype(F32)).astype(BF16)
    loop(1, 16, lambda d: give_back_in(d).wait_recv())
    v = back[...].astype(F32).reshape(16, 2, 8, 512)
    first = (((0,), (0,)), ((), ()))
    for q in range(2):
        rows = v[:, q].reshape(128, 512).astype(BF16)
        mix = dot(w_hi, rows, first) + dot(w_lo, rows, first)
        for z in range(4):
            own_d[4 * q + z] = own_d[4 * q + z] + mix[:, lanes(z)]
    rs2_out[...] = own_d[...].astype(BF16)

    def scatter2(d):
        return send(
            rs2_out.at[z_block(d)], rs2_in.at[d - 1], sz.at[d + 13], rz.at[d + 13], E, tp_at(d)
        )

    loop(1, 8, lambda d: scatter2(d).start())
    total = own_d[Z] + rm[C, Z].astype(F32)
    loop(1, 8, lambda d: scatter2(d).wait_recv())
    for d in range(7):
        total = total + rs2_in[d].astype(F32)
    lout[...] = total.astype(BF16)
    done = pltpu.make_async_copy(lout, layer_out, store_sem.at[2])
    done.start()

    for f in (w_p, w_q, n_p, n_q, back_p, back_q):
        loop(1, 4, lambda d, f=f: f(d).wait_send())
    for f in (scatter, gather, scatter2):
        loop(1, 8, lambda d, f=f: f(d).wait_send())
    for f in (dispatch, give_back):
        loop(1, 16, lambda d, f=f: f(d).wait_send())
    loop(0, 16, lambda d: forward(d).wait_send())
    for s in (swap_mixer, swap_resid, swap_dense, swap_expert):
        s.wait_send()
    keep_state.wait()
    keep_conv.wait()
    done.wait()


SCRATCH = [
    ((32, 2048), BF16),
    ((16, 128), F32),
    ((16, 128), F32),
    ((16, 128), F32),
    ((16, 128), BF16),
    ((3, 4, 128), F32),
    ((32, 2048), BF16),
    ((2, 32), jnp.int32),
    ((2, 32), F32),
    ((3, 3, 32, 128), BF16),
    ((32, 2, 64, 128), F32),
    ((4, 128, 256), BF16),
    ((4, 128, 256), BF16),
    ((128, 2048), BF16),
    ((2, 2048, 256), BF16),
    ((2, 128, 2048), BF16),
    ((2048, 256), BF16),
    ((128, 2048), BF16),
    ((32, 2048), BF16),
    ((4, 32, 512), BF16),
    ((4, 32, 512), BF16),
    ((4, 32, 512), BF16),
    ((4, 32, 512), BF16),
    ((4, 32, 256), BF16),
    ((4, 32, 256), BF16),
    ((3, 32, 256), BF16),
    ((3, 32, 256), BF16),
    ((2, 32, 128), F32),
    ((32, 128), F32),
    ((32, 128), F32),
    ((32, 128), F32),
    ((32, 128), F32),
    ((3, 32, 128), BF16),
    ((2, 8, 32, 128), BF16),
    ((8, 32, 128), F32),
    ((8, 32, 128), BF16),
    ((8, 32, 128), BF16),
    ((7, 32, 128), BF16),
    ((2, 8, 32, 128), BF16),
    ((8, 128), F32),
    ((2, 128, 32), F32),
    ((16, 16, 512), BF16),
    ((2, 16, 16, 512), BF16),
    ((128, 2048), BF16),
    ((2, 2, 128, 512), BF16),
    ((2, 128, 512), F32),
    ((2, 128, 512), BF16),
    ((16, 16, 512), BF16),
    ((16, 16, 512), BF16),
    ((32, 2048), BF16),
    ((2, 8, 32, 128), BF16),
    ((8, 32, 128), F32),
    ((8, 32, 128), BF16),
    ((8, 32, 128), BF16),
    ((7, 32, 128), BF16),
    ((32, 128), BF16),
]


def on_device(*args):
    (
        residual,
        mixer_gain,
        gate_proj,
        input_proj,
        write_proj,
        read_proj,
        step_proj,
        conv_weight,
        step_bias,
        log_rate,
        skip_gain,
        group_gain,
        ssm_state,
        conv_state,
        out_proj,
        ffn_gain,
        routes,
        route_weight,
        expert_gate,
        expert_up,
        expert_down,
        dense_gate,
        dense_up,
        dense_down,
        blend_weight,
    ) = args
    conv_t = jnp.transpose(conv_state, (1, 2, 0, 3))
    layer_out, new_state, newest = pl.pallas_call(
        kernel,
        out_shape=(
            jax.ShapeDtypeStruct((32, 128), BF16),
            jax.ShapeDtypeStruct((32, 2, 64, 128), F32),
            jax.ShapeDtypeStruct((3, 32, 128), BF16),
        ),
        in_specs=[ANY] * 8 + [SMEM] * 3 + [ANY] * 14,
        out_specs=(ANY, ANY, ANY),
        scratch_shapes=[pltpu.VMEM(s, d) for s, d in SCRATCH]
        + [
            pltpu.SemaphoreType.DMA((24,)),
            pltpu.SemaphoreType.DMA((3,)),
            pltpu.SemaphoreType.DMA((12,)),
            pltpu.SemaphoreType.DMA((12,)),
            pltpu.SemaphoreType.DMA((6,)),
            pltpu.SemaphoreType.DMA((6,)),
            pltpu.SemaphoreType.DMA((21,)),
            pltpu.SemaphoreType.DMA((21,)),
            pltpu.SemaphoreType.DMA((4,)),
            pltpu.SemaphoreType.DMA((4,)),
            pltpu.SemaphoreType.DMA((15,)),
            pltpu.SemaphoreType.DMA((15,)),
            pltpu.SemaphoreType.DMA((16,)),
            pltpu.SemaphoreType.DMA((16,)),
            pltpu.SemaphoreType.DMA((15,)),
            pltpu.SemaphoreType.DMA((15,)),
        ],
        compiler_params=pltpu.CompilerParams(
            collective_id=0, has_side_effects=True, vmem_limit_bytes=40 * 1024 * 1024
        ),
    )(
        residual,
        mixer_gain.reshape(16, 128),
        gate_proj,
        input_proj,
        write_proj,
        read_proj,
        step_proj.T,
        jnp.transpose(conv_weight, (1, 0, 2)),
        step_bias,
        log_rate,
        skip_gain,
        group_gain.reshape(16, 128),
        ssm_state,
        conv_t,
        out_proj,
        ffn_gain.reshape(16, 128),
        routes.T,
        route_weight.T,
        expert_gate,
        expert_up,
        expert_down,
        dense_gate,
        dense_up,
        dense_down,
        blend_weight.reshape(16, 128),
    )
    new_conv = jnp.concatenate([conv_t[1:], newest[None]], axis=0)
    return layer_out, new_state, jnp.transpose(new_conv, (2, 0, 1, 3))


def solution(mesh):
    return jax.shard_map(
        on_device,
        mesh=mesh,
        in_specs=(
            P("ep", None),
            P(),
            P("ep", "tp"),
            P("ep", "tp"),
            P("ep", "tp"),
            P("ep", "tp"),
            P(),
            P(),
            P(),
            P(),
            P(),
            P(),
            P("ep", "tp", None, None),
            P("ep", None, None, "tp"),
            P("tp", None),
            P(),
            P("ep", None),
            P("ep", None),
            P("ep", None, "tp"),
            P("ep", None, "tp"),
            P("ep", "tp", None),
            P(None, "tp"),
            P(None, "tp"),
            P("tp", None),
            P(),
        ),
        out_specs=(P("ep", "tp"), P("ep", "tp", None, None), P("ep", None, None, "tp")),
        check_vma=False,
    )
```

time: 147 us -> 85.7 us (0.58)
  waiting for transfers between devices: 63.2 us -> 0 us
  Pallas kernels: 0 us -> 59.1 us
  starting transfers between devices: 30.6 us -> 0 us
  blocking collectives: 28.1 us -> 0 us
  local copies, waits for them, and re-layouts: 7.97 us -> 24.1 us
  matrix products: 8.09 us -> 0 us
  other arithmetic: 7.2 us -> 0.64 us
    all_to_all x6 -> x0, waiting for transfers between devices: 63.2 us -> none  [the longest x2 23.5 us: sum_at_owner(): lax.all_to_all(parts, axis, split_axis=0, concat_axis=0, tiled=True)]
    pallas_call x0 -> x1, Pallas kernels: none -> 59.1 us  [on_device(): pl.pallas_call(kernel, out_shape=(jax.ShapeDtypeStruct((32, 128), BF16),...]
    all_to_all x6 -> x0, starting transfers between devices: 30.6 us -> none  [the longest x2 15.6 us: sum_at_owner(): lax.all_to_all(parts, axis, split_axis=0, concat_axis=0, tiled=True)]
    all_to_all x2 -> x0, blocking collectives: 28.1 us -> none  [the longest x1 14.2 us: on_device(): lax.all_to_all(normed, 'ep', split_axis=1, concat_axis=0, tiled=True)]
    unnamed x43 -> x52, local copies, waits for them, and re-layouts: 1.54 us -> 24 us
    dot_general x11 -> x0, matrix products: 8.09 us -> none  [the longest x1 2.06 us: on_device(): jnp.dot(pieces, joined, preferred_element_type=jnp.float32)]
    add x3 -> x0, other arithmetic: 2.12 us -> none  [the longest x1 2.02 us: on_device(): decay_factor[:, :, None, None] * ssm_state]
    reduce_sum x8 -> x0, other arithmetic: 2.01 us -> none  [the longest x2 1.27 us: rms_rows(): jnp.mean(floats_in * floats_in, axis=-1, keepdims=True) + epsilon]
  transfers between devices with their start and end apart: 6 -> 0, of which waited for: 6 -> 0; matrix products, arithmetic and copies ran while one was open for 4% -> 0% of each run, Pallas kernels for 0% -> 0%
where the time goes in v1:
time: 85.7 us; the launch traced here: 84.4 us
  Pallas kernels  59.1 us (69%)
  local copies, waits for them, and re-layouts  24.1 us (28%)
    pallas_call x1, Pallas kernels, on_device(): pl.pallas_call(kernel, out_shape=(jax.ShapeDtypeStruct((32, 128), BF16),...  59.1 us
    unnamed x52, local copies, waits for them, and re-layouts  24 us

profile of v1, /device:TPU:1, one launch (start us, length us, event | category | flops | bytes accessed | tf_op | source)
XLA Modules:
  0.0 84.4 jit_solution(6575407233181428767)
XLA Ops:
  0.6 1.6 %copy-done = f32[32,2,64,128]{3,2,1,0:T(8,128)S(1)} copy-done((f32[32,2,64,128]{3,2,1,0:T(8,128)S(1)}, f32[32,2,64,128]{3,2,1,0:T(8,128)}, u32[]{:S(2)}) %copy-start) | copy-done | bytes 2097176
  2.2 1.2 %copy-done.1 = bf16[2,2048,128]{2,1,0:T(8,128)(2,1)S(1)} copy-done((bf16[2,2048,128]{2,1,0:T(8,128)(2,1)S(1)}, bf16[2,2048,128]{2,1,0:T(8,128)(2,1)}, u32[]{:S(2)}) %copy-start.1) | copy-done | bytes 1048600
  3.5 1.2 %copy-done.2 = bf16[2,2048,128]{2,1,0:T(8,128)(2,1)S(1)} copy-done((bf16[2,2048,128]{2,1,0:T(8,128)(2,1)S(1)}, bf16[2,2048,128]{2,1,0:T(8,128)(2,1)}, u32[]{:S(2)}) %copy-start.2) | copy-done | bytes 1048600
  4.7 1.2 %copy-done.3 = bf16[2,128,2048]{2,1,0:T(8,128)(2,1)S(1)} copy-done((bf16[2,128,2048]{2,1,0:T(8,128)(2,1)S(1)}, bf16[2,128,2048]{2,1,0:T(8,128)(2,1)}, u32[]{:S(2)}) %copy-start.3) | copy-done | bytes 1048600
  5.9 1.0 %copy-done.4 = bf16[128,2048]{1,0:T(8,128)(2,1)S(1)} copy-done((bf16[128,2048]{1,0:T(8,128)(2,1)S(1)}, bf16[128,2048]{1,0:T(8,128)(2,1)}, u32[]{:S(2)}) %copy-start.4) | copy-done | bytes 524312
  7.0 1.0 %copy-done.5 = bf16[2048,128]{1,0:T(8,128)(2,1)S(1)} copy-done((bf16[2048,128]{1,0:T(8,128)(2,1)S(1)}, bf16[2048,128]{1,0:T(8,128)(2,1)}, u32[]{:S(2)}) %copy-start.5) | copy-done | bytes 524312
  8.0 1.0 %copy-done.6 = bf16[2048,128]{1,0:T(8,128)(2,1)S(1)} copy-done((bf16[2048,128]{1,0:T(8,128)(2,1)S(1)}, bf16[2048,128]{1,0:T(8,128)(2,1)}, u32[]{:S(2)}) %copy-start.6) | copy-done | bytes 524312
  9.0 1.0 %copy-done.7 = bf16[128,2048]{1,0:T(8,128)(2,1)S(1)} copy-done((bf16[128,2048]{1,0:T(8,128)(2,1)S(1)}, bf16[128,2048]{1,0:T(8,128)(2,1)}, u32[]{:S(2)}) %copy-start.7) | copy-done | bytes 524312
  10.1 0.9 %copy-done.8 = bf16[32,3,3,128]{3,0,2,1:T(8,128)(2,1)S(1)} copy-done((bf16[32,3,3,128]{3,0,2,1:T(8,128)(2,1)S(1)}, bf16[32,3,3,128]{3,0,2,1:T(8,128)(2,1)}, u32[]{:S(2)}) %copy-start.8) | copy-done | bytes 73752
  11.0 0.9 %copy-done.9 = bf16[32,2048]{1,0:T(8,128)(2,1)S(1)} copy-done((bf16[32,2048]{1,0:T(8,128)(2,1)S(1)}, bf16[32,2048]{1,0:T(8,128)(2,1)}, u32[]{:S(2)}) %copy-start.9) | copy-done | bytes 131096
  11.9 0.9 %copy-done.10 = bf16[2048,32]{0,1:T(8,128)(2,1)S(1)} copy-done((bf16[2048,32]{0,1:T(8,128)(2,1)S(1)}, bf16[2048,32]{0,1:T(8,128)(2,1)}, u32[]{:S(2)}) %copy-start.10) | copy-done | bytes 131096
  12.8 0.9 %copy-done.11 = f32[4,3,2048]{2,0,1:T(4,128)S(1)} copy-done((f32[4,3,2048]{2,0,1:T(4,128)S(1)}, f32[4,3,2048]{2,0,1:T(4,128)}, u32[]{:S(2)}) %copy-start.11) | copy-done | bytes 98328
  13.7 0.8 copy-done.12
  14.4 0.8 copy-done.13
  15.2 0.8 copy-done.14
  15.9 0.8 copy-done.15
  16.7 0.7 copy-done.16
  17.4 0.7 copy-done.17
  18.1 0.7 copy-done.18
  18.8 0.7 copy-done.19
  19.5 0.7 copy-done.20
  20.2 0.7 copy-done.21
  22.8 59.1 %shard_map.256 = (bf16[32,128]{1,0:T(8,128)(2,1)S(1)}, f32[32,2,64,128]{3,2,1,0:T(8,128)S(1)}, bf16[3,32,128]{2,1,0:T(8,128)(2,1)S(1)}) custom-call(bf16[32,2048]{1,0:T(8,128)(2,1)S(1)} %copy-done.9, f32[16,128]{1,0:T(8,128)S(1)} %bitcast.17, bf16[128,128]{1,0:T(8,128)(2,1)S(1)} %copy-done.12, bf16[128,128]{1,0:T(8,128)(2,1)S(1)} %copy-done.13, ...), custom_call_target="tpu_custom_call" | custom-call | tf_op jit(solution)/shard_map/pallas_call | solution.py:647
  83.1 1.3 %copy.31 = f32[32,2,64,128]{3,2,1,0:T(8,128)} copy(f32[32,2,64,128]{3,2,1,0:T(8,128)S(1)} %get-tuple-element.13) | data formatting | bytes 4194304
  (31 shorter events, 3.2 us)
Async XLA Ops:
  0.6 1.6 %copy-start = (f32[32,2,64,128]{3,2,1,0:T(8,128)S(1)}, f32[32,2,64,128]{3,2,1,0:T(8,128)}, u32[]{:S(2)}) copy-start(f32[32,2,64,128]{3,2,1,0:T(8,128)} %ssm_state.1) | copy-start | bytes 6291460
  2.2 1.2 %copy-start.1 = (bf16[2,2048,128]{2,1,0:T(8,128)(2,1)S(1)}, bf16[2,2048,128]{2,1,0:T(8,128)(2,1)}, u32[]{:S(2)}) copy-start(bf16[2,2048,128]{2,1,0:T(8,128)(2,1)} %expert_gate.1) | copy-start | bytes 3145732
  3.5 1.2 %copy-start.2 = (bf16[2,2048,128]{2,1,0:T(8,128)(2,1)S(1)}, bf16[2,2048,128]{2,1,0:T(8,128)(2,1)}, u32[]{:S(2)}) copy-start(bf16[2,2048,128]{2,1,0:T(8,128)(2,1)} %expert_up.1) | copy-start | bytes 3145732
  4.7 1.2 %copy-start.3 = (bf16[2,128,2048]{2,1,0:T(8,128)(2,1)S(1)}, bf16[2,128,2048]{2,1,0:T(8,128)(2,1)}, u32[]{:S(2)}) copy-start(bf16[2,128,2048]{2,1,0:T(8,128)(2,1)} %expert_down.1) | copy-start | bytes 3145732
  5.9 1.0 %copy-start.4 = (bf16[128,2048]{1,0:T(8,128)(2,1)S(1)}, bf16[128,2048]{1,0:T(8,128)(2,1)}, u32[]{:S(2)}) copy-start(bf16[128,2048]{1,0:T(8,128)(2,1)} %out_proj.1) | copy-start | bytes 1572868
  6.9 1.0 %copy-start.5 = (bf16[2048,128]{1,0:T(8,128)(2,1)S(1)}, bf16[2048,128]{1,0:T(8,128)(2,1)}, u32[]{:S(2)}) copy-start(bf16[2048,128]{1,0:T(8,128)(2,1)} %dense_gate.1) | copy-start | bytes 1572868
  8.0 1.0 %copy-start.6 = (bf16[2048,128]{1,0:T(8,128)(2,1)S(1)}, bf16[2048,128]{1,0:T(8,128)(2,1)}, u32[]{:S(2)}) copy-start(bf16[2048,128]{1,0:T(8,128)(2,1)} %dense_up.1) | copy-start | bytes 1572868
  9.0 1.0 %copy-start.7 = (bf16[128,2048]{1,0:T(8,128)(2,1)S(1)}, bf16[128,2048]{1,0:T(8,128)(2,1)}, u32[]{:S(2)}) copy-start(bf16[128,2048]{1,0:T(8,128)(2,1)} %dense_down.1) | copy-start | bytes 1572868
  10.1 0.9 %copy-start.8 = (bf16[32,3,3,128]{3,0,2,1:T(8,128)(2,1)S(1)}, bf16[32,3,3,128]{3,0,2,1:T(8,128)(2,1)}, u32[]{:S(2)}) copy-start(bf16[32,3,3,128]{3,0,2,1:T(8,128)(2,1)} %param.38) | copy-start | bytes 221188
  11.0 0.9 %copy-start.9 = (bf16[32,2048]{1,0:T(8,128)(2,1)S(1)}, bf16[32,2048]{1,0:T(8,128)(2,1)}, u32[]{:S(2)}) copy-start(bf16[32,2048]{1,0:T(8,128)(2,1)} %residual.1) | copy-start | bytes 393220
  11.9 0.9 %copy-start.10 = (bf16[2048,32]{0,1:T(8,128)(2,1)S(1)}, bf16[2048,32]{0,1:T(8,128)(2,1)}, u32[]{:S(2)}) copy-start(bf16[2048,32]{0,1:T(8,128)(2,1)} %param.31) | copy-start | bytes 393220
  12.8 0.9 %copy-start.11 = (f32[4,3,2048]{2,0,1:T(4,128)S(1)}, f32[4,3,2048]{2,0,1:T(4,128)}, u32[]{:S(2)}) copy-start(f32[4,3,2048]{2,0,1:T(4,128)} %param.32) | copy-start | bytes 294916
  13.7 0.8 copy-start.12
  14.4 0.8 copy-start.13
  15.2 0.8 copy-start.14
  15.9 0.8 copy-start.15
  16.7 0.7 copy-start.16
  17.4 0.7 copy-start.17
  18.1 0.7 copy-start.18
  18.8 0.7 copy-start.19
  19.5 0.7 copy-start.20
  20.2 0.7 copy-start.21
  20.8 0.7 copy-start.22
  21.5 0.7 copy-start.23
  (1 other events, 0.7 us)

commit v2 on v1

--- a/solution.py
+++ b/solution.py
@@ -673,7 +673,7 @@
             pltpu.SemaphoreType.DMA((15,)),
         ],
         compiler_params=pltpu.CompilerParams(
-            collective_id=0, has_side_effects=True, vmem_limit_bytes=40 * 1024 * 1024
+            collective_id=0, has_side_effects=True, vmem_limit_bytes=67043328
         ),
     )(
         residual,

time: 85.7 us -> 67.1 us (0.78)
  local copies, waits for them, and re-layouts: 24.1 us -> 5.26 us
    unnamed x52 -> x2, local copies, waits for them, and re-layouts: 24 us -> 4.45 us
where the time goes in v2:
time: 67.1 us; the launch traced here: 66.7 us
  Pallas kernels  59.4 us (89%)
  local copies, waits for them, and re-layouts  5.26 us (8%)
  other arithmetic  1.38 us (2%)
    pallas_call x1, Pallas kernels, on_device(): pl.pallas_call(kernel, out_shape=(jax.ShapeDtypeStruct((32, 128), BF16),...  59.4 us
    unnamed x2, local copies, waits for them, and re-layouts  4.45 us
    transpose x1, other arithmetic, on_device(): return (layer_out, new_state, jnp.transpose(new_conv, (2, 0, 1, 3)))  1.38 us

profile of v2, /device:TPU:1, one launch (start us, length us, event | category | flops | bytes accessed | tf_op | source)
XLA Modules:
  0.0 66.7 jit_solution(1979850644041377713)
XLA Ops:
  0.6 59.4 %shard_map.256 = (bf16[32,128]{1,0:T(8,128)(2,1)}, f32[32,2,64,128]{3,2,1,0:T(8,128)}, bf16[3,32,128]{2,1,0:T(8,128)(2,1)}) custom-call(bf16[32,2048]{1,0:T(8,128)(2,1)} %residual.1, f32[16,128]{1,0:T(8,128)} %bitcast.17, bf16[128,128]{1,0:T(8,128)(2,1)} %gate_proj.1, bf16[128,128]{1,0:T(8,128)(2,1)} %input_proj.1, bf16[128,128]{1,0:T(8,128)(2,1)} %write_proj.1, ...), custom_call_target="tpu_custom_call" | custom-call | tf_op jit(solution)/shard_map/pallas_call | solution.py:647
  60.0 0.8 %slice.4 = bf16[2,3,32,128]{3,2,1,0:T(8,128)(2,1)S(1)} slice(bf16[3,3,32,128]{3,2,1,0:T(8,128)(2,1)} %bitcast.13), slice={[1:3], [0:3], [0:32], [0:128]} | slice | bytes 98304 | tf_op jit(solution)/shard_map/slice | solution.py:705
  60.8 1.4 %maximum_bitcast_fusion = bf16[32,3,3,128]{3,0,2,1:T(8,128)(2,1)} fusion(bf16[1,3,32,128]{3,2,1,0:T(8,128)(2,1)} %bitcast.16, bf16[2,3,32,128]{3,2,1,0:T(8,128)(2,1)S(1)} %slice.4), kind=kLoop, calls=%fused_computation | loop fusion | flops 36864 | bytes 147456 | tf_op jit(solution)/shard_map/transpose | solution.py:706
  62.2 1.3 %copy.30 = bf16[32,128]{1,0:T(8,128)(2,1)} copy(bf16[32,128]{1,0:T(8,128)(2,1)} %get-tuple-element.12) | data formatting | bytes 16384
  63.5 3.2 %copy.31 = f32[32,2,64,128]{3,2,1,0:T(8,128)} copy(f32[32,2,64,128]{3,2,1,0:T(8,128)} %get-tuple-element.13) | data formatting | bytes 4194304

commit v3 on v2

--- a/solution.py
+++ b/solution.py
@@ -11,8 +11,9 @@
 F32 = jnp.float32
 BF16 = jnp.bfloat16
 EPS = 1e-06
+VM = pl.BlockSpec(memory_space=pltpu.VMEM)
 ANY = pl.BlockSpec(memory_space=pl.ANY)
-SMEM = pl.BlockSpec(memory_space=pltpu.SMEM)
+HBM = pl.BlockSpec(memory_space=pltpu.HBM)
 
 
 def dot(a, b, dims=(((1,), (0,)), ((), ()))):
@@ -55,18 +56,21 @@
     blend_weight,
     layer_out,
     new_state,
-    newest,
+    new_conv,
     res,
     mgain,
     ggain,
     fgain,
     blend,
     cw,
+    heads,
     sproj,
     rts,
     rw,
     cst,
     st,
+    st_hi,
+    st_lo,
     wp,
     wq,
     op,
@@ -86,16 +90,12 @@
     dec,
     dxs,
     bs,
-    cs,
-    ys,
-    nw,
     mixer_half,
     mixer_own,
     mixer_pair,
     rs_out,
     rs_in,
     rm,
-    rmf_own,
     place,
     outb,
     rx,
@@ -111,9 +111,7 @@
     pair_d,
     rs2_out,
     rs2_in,
-    lout,
     load_sem,
-    store_sem,
     s1,
     r1,
     s2,
@@ -204,6 +202,9 @@
     load(
         "small",
         (step_proj, sproj),
+        (step_bias, heads.at[0]),
+        (log_rate, heads.at[1]),
+        (skip_gain, heads.at[2]),
         (conv_weight.at[:, :, chan], cw),
         (conv_state, cst),
         (routes, rts),
@@ -268,20 +269,23 @@
     raw = dot(nat[...], sproj[...], (((1,), (1,)), ((), ())))
     lane32 = lax.broadcasted_iota(jnp.int32, (32, 32), 1)
     lane128 = lax.broadcasted_iota(jnp.int32, (32, 128), 1)
-    dts = []
+    head_row = lane32[0:1]
+
+    def of_head(i, h):
+        return jnp.sum(jnp.where(head_row == 2 * T + h, heads[i], 0.0), axis=1, keepdims=True)
+
+    dts, decays = [], []
     for h in range(2):
         col = jnp.sum(jnp.where(lane32 == 2 * T + h, raw, 0.0), axis=1, keepdims=True)
-        v = jnp.broadcast_to(col, (32, 128)) + step_bias[2 * T + h]
+        v = jnp.broadcast_to(col, (32, 128)) + of_head(0, h)
         dt = jnp.maximum(v, 0.0) + jnp.log1p(jnp.exp(-jnp.abs(v)))
-        rate = jnp.exp(jnp.full((32, 128), log_rate[2 * T + h], F32))
-        dec[h] = jnp.exp(-rate * dt)
+        rate = jnp.exp(jnp.broadcast_to(of_head(1, h), (32, 128)))
+        decays.append(jnp.exp(-rate * dt))
+        dec[h] = decays[h]
         dts.append(dt)
     dt = jnp.where(lane128 < 64, dts[0], dts[1])
-    skip = jnp.where(
-        lane128 < 64,
-        jnp.full((32, 128), skip_gain[2 * T], F32),
-        jnp.full((32, 128), skip_gain[2 * T + 1], F32),
-    )
+    decay = jnp.where(lane128 < 64, decays[0], decays[1])
+    skip = jnp.where(lane128 < 64, of_head(2, 0), of_head(2, 1))
     held = []
     for c in range(3):
         acc = cst[0, c].astype(F32) * cw[c, 0:1, :]
@@ -301,6 +305,19 @@
     place[0] = spots[0] + spots[1]
     place[1] = spots[0] * rw[0:1, :] + spots[1] * rw[1:2, :]
 
+    loaded("state")
+
+    def split(s):
+        v = st[s].reshape(128, 128)
+        hi = v.astype(BF16)
+        st_hi[s] = hi
+        st_lo[s] = (v - hi.astype(F32)).astype(BF16)
+
+    loop(0, 32, split)
+    for k in range(2):
+        for c in range(3):
+            new_conv[k, c] = cst[k + 1, c]
+
     loop(1, 4, lambda d: w_p(d).wait_recv())
     loop(1, 4, lambda d: n_p(d).wait_recv())
     part_p = dot(rp[...].reshape(128, 512), wp[...].reshape(512, 256))
@@ -324,7 +341,7 @@
 
     loop(1, 4, lambda d: back_q(d).start())
     own_p, own_q = part_p[0:32], part_q[0:32]
-    loaded("state", "op")
+    loaded("op")
     loop(1, 4, lambda d: back_p(d).wait_recv())
     for d in range(3):
         own_p = own_p + r2p[d].astype(F32)
@@ -336,35 +353,47 @@
     acts = []
     for c in range(3):
         row = fresh[c].astype(BF16)
-        nw[c] = row
+        new_conv[2, c] = row
         acts.append(silu(held[c] + row.astype(F32) * cw[c, 3:4, :]))
     x_act = acts[0]
-    dxs[...] = dt * x_act
-    bs[...] = acts[1]
-    cs[...] = acts[2]
-
-    lane_y = lax.broadcasted_iota(jnp.int32, (64, 128), 1)
+
+    write, read = acts[1], acts[2]
+    read_hi = read.astype(BF16)
+    read_lo = (read - read_hi.astype(F32)).astype(BF16)
+    last = (((1,), (1,)), ((), ()))
+    sub8 = lax.broadcasted_iota(jnp.int32, (8, 128), 0)
+    outs = []
+    for g in range(4):
+        eight = slice(8 * g, 8 * g + 8)
+        hi = st_hi[eight].reshape(1024, 128)
+        lo = st_lo[eight].reshape(1024, 128)
+        two = jnp.concatenate([read_hi[eight], read_lo[eight]], axis=0)
+        r = dot(two, hi, last)
+        r = r[0:8] + r[8:16] + dot(read_hi[eight], lo, last)
+        y = jnp.zeros((8, 128), F32)
+        for i in range(8):
+            y = jnp.where(sub8 == i, r[:, lanes(i)], y)
+        outs.append(y)
+    step_x = dt * x_act
+    ssm_out = decay * jnp.concatenate(outs, axis=0) + step_x * jnp.sum(
+        write * read, axis=1, keepdims=True
+    )
+    dxs[...] = step_x
+    bs[...] = write
 
     def tokens(g):
         base = pl.multiple_of(g * 8, 8)
         dx_t = jnp.transpose(dxs[pl.ds(base, 8), :])
-        yt = [jnp.zeros((64, 128), F32), jnp.zeros((64, 128), F32)]
         for i in range(8):
             s = base + i
             b_row = bs[pl.ds(s, 1), :]
-            c_row = cs[pl.ds(s, 1), :]
             for h in range(2):
-                ns = dec[h, pl.ds(s, 1), :] * st[s, h] + dx_t[h * 64 : h * 64 + 64, i : i + 1] * b_row
-                st[s, h] = ns
-                y = jnp.sum(ns * c_row, axis=1, keepdims=True)
-                yt[h] = jnp.where(lane_y == i, y, yt[h])
-        ys[pl.ds(base, 8), :] = jnp.transpose(jnp.concatenate(yt, axis=0))[0:8]
-
-    loop(0, 4, tokens)
-    keep_state = pltpu.make_async_copy(st, new_state, store_sem.at[0])
-    keep_conv = pltpu.make_async_copy(nw, newest, store_sem.at[1])
-
-    gated = (ys[...] + skip * x_act) * silu(z_proj)
+                new_state[s, h] = (
+                    dec[h, pl.ds(s, 1), :] * st[s, h]
+                    + dx_t[h * 64 : h * 64 + 64, i : i + 1] * b_row
+                )
+
+    gated = (ssm_out + skip * x_act) * silu(z_proj)
     gated = gated * lax.rsqrt(jnp.mean(gated * gated, axis=-1, keepdims=True) + EPS)
     mixed = (gated * ggain[pl.ds(T, 1), :]).astype(BF16)
     part = dot(mixed, op[...])
@@ -378,8 +407,6 @@
 
     swap_mixer = to_pair(mixer_half.at[1 - C], mixer_pair, 0)
     swap_mixer.start()
-    keep_state.start()
-    keep_conv.start()
     swap_mixer.wait_recv()
     mixer_own[...] = mixer_own[...] + mixer_pair[...].astype(F32)
     rs_out[...] = mixer_own[...].astype(BF16)
@@ -394,6 +421,7 @@
 
     loop(1, 8, lambda d: scatter(d).start())
     total = mixer_own[Z]
+    loop(0, 2, tokens)
     resid_cols = res[:, chan].astype(F32)
     loop(1, 8, lambda d: scatter(d).wait_recv())
     for d in range(7):
@@ -411,6 +439,7 @@
         )
 
     loop(1, 8, lambda d: gather(d).start())
+    loop(2, 4, tokens)
     loaded("dense", "experts", "ffn")
     loop(1, 8, lambda d: gather_in(d).wait_recv())
     swap_resid = to_pair(rm.at[C], rm.at[C], 1)
@@ -537,9 +566,7 @@
     loop(1, 8, lambda d: scatter2(d).wait_recv())
     for d in range(7):
         total = total + rs2_in[d].astype(F32)
-    lout[...] = total.astype(BF16)
-    done = pltpu.make_async_copy(lout, layer_out, store_sem.at[2])
-    done.start()
+    layer_out[...] = total.astype(BF16)
 
     for f in (w_p, w_q, n_p, n_q, back_p, back_q):
         loop(1, 4, lambda d, f=f: f(d).wait_send())
@@ -550,9 +577,17 @@
     loop(0, 16, lambda d: forward(d).wait_send())
     for s in (swap_mixer, swap_resid, swap_dense, swap_expert):
         s.wait_send()
-    keep_state.wait()
-    keep_conv.wait()
-    done.wait()
+
+
+def write_out(a, b, c, a_out, b_out, c_out, sem):
+    copies = [
+        pltpu.make_async_copy(src, dst, sem.at[i])
+        for i, (src, dst) in enumerate(((b, b_out), (c, c_out), (a, a_out)))
+    ]
+    for copy in copies:
+        copy.start()
+    for copy in copies:
+        copy.wait()
 
 
 SCRATCH = [
@@ -562,11 +597,14 @@
     ((16, 128), F32),
     ((16, 128), BF16),
     ((3, 4, 128), F32),
+    ((3, 1, 32), F32),
     ((32, 2048), BF16),
     ((2, 32), jnp.int32),
     ((2, 32), F32),
     ((3, 3, 32, 128), BF16),
     ((32, 2, 64, 128), F32),
+    ((32, 128, 128), BF16),
+    ((32, 128, 128), BF16),
     ((4, 128, 256), BF16),
     ((4, 128, 256), BF16),
     ((128, 2048), BF16),
@@ -586,16 +624,12 @@
     ((2, 32, 128), F32),
     ((32, 128), F32),
     ((32, 128), F32),
-    ((32, 128), F32),
-    ((32, 128), F32),
-    ((3, 32, 128), BF16),
     ((2, 8, 32, 128), BF16),
     ((8, 32, 128), F32),
     ((8, 32, 128), BF16),
     ((8, 32, 128), BF16),
     ((7, 32, 128), BF16),
     ((2, 8, 32, 128), BF16),
-    ((8, 128), F32),
     ((2, 128, 32), F32),
     ((16, 16, 512), BF16),
     ((2, 16, 16, 512), BF16),
@@ -611,7 +645,6 @@
     ((8, 32, 128), BF16),
     ((8, 32, 128), BF16),
     ((7, 32, 128), BF16),
-    ((32, 128), BF16),
 ]
 
 
@@ -644,19 +677,18 @@
         blend_weight,
     ) = args
     conv_t = jnp.transpose(conv_state, (1, 2, 0, 3))
-    layer_out, new_state, newest = pl.pallas_call(
+    results = pl.pallas_call(
         kernel,
         out_shape=(
-            jax.ShapeDtypeStruct((32, 128), BF16),
-            jax.ShapeDtypeStruct((32, 2, 64, 128), F32),
-            jax.ShapeDtypeStruct((3, 32, 128), BF16),
+            pltpu.VMEM((32, 128), BF16),
+            pltpu.VMEM((32, 2, 64, 128), F32),
+            pltpu.VMEM((3, 3, 32, 128), BF16),
         ),
-        in_specs=[ANY] * 8 + [SMEM] * 3 + [ANY] * 14,
-        out_specs=(ANY, ANY, ANY),
+        in_specs=[HBM] * 25,
+        out_specs=(VM, VM, VM),
         scratch_shapes=[pltpu.VMEM(s, d) for s, d in SCRATCH]
         + [
-            pltpu.SemaphoreType.DMA((24,)),
-            pltpu.SemaphoreType.DMA((3,)),
+            pltpu.SemaphoreType.DMA((25,)),
             pltpu.SemaphoreType.DMA((12,)),
             pltpu.SemaphoreType.DMA((12,)),
             pltpu.SemaphoreType.DMA((6,)),
@@ -673,7 +705,7 @@
             pltpu.SemaphoreType.DMA((15,)),
         ],
         compiler_params=pltpu.CompilerParams(
-            collective_id=0, has_side_effects=True, vmem_limit_bytes=67043328
+            collective_id=0, has_side_effects=True, vmem_limit_bytes=64_400_000
         ),
     )(
         residual,
@@ -684,9 +716,9 @@
         read_proj,
         step_proj.T,
         jnp.transpose(conv_weight, (1, 0, 2)),
-        step_bias,
-        log_rate,
-        skip_gain,
+        step_bias.reshape(1, 32),
+        log_rate.reshape(1, 32),
+        skip_gain.reshape(1, 32),
         group_gain.reshape(16, 128),
         ssm_state,
         conv_t,
@@ -702,7 +734,14 @@
         dense_down,
         blend_weight.reshape(16, 128),
     )
-    new_conv = jnp.concatenate([conv_t[1:], newest[None]], axis=0)
+    layer_out, new_state, new_conv = pl.pallas_call(
+        write_out,
+        out_shape=tuple(jax.ShapeDtypeStruct(r.shape, r.dtype) for r in results),
+        in_specs=[ANY] * 3,
+        out_specs=(HBM,) * 3,
+        scratch_shapes=[pltpu.SemaphoreType.DMA((3,))],
+        compiler_params=pltpu.CompilerParams(vmem_limit_bytes=1 << 20),
+    )(*results)
     return layer_out, new_state, jnp.transpose(new_conv, (2, 0, 1, 3))
 
 

time: 67.1 us -> 55.3 us (0.82)
  local copies, waits for them, and re-layouts: 5.26 us -> 0 us
  Pallas kernels: 59.4 us -> 54.2 us
  other arithmetic: 1.38 us -> 0 us
    pallas_call x1 -> x2, Pallas kernels: 59.4 us -> 54.2 us  [the longest x1 52.8 us: on_device(): pl.pallas_call(kernel, out_shape=(pltpu.VMEM((32, 128), BF16), pltpu.VMEM...]
    unnamed x2 -> x0, local copies, waits for them, and re-layouts: 4.45 us -> none
    transpose x1 -> x0, other arithmetic: 1.38 us -> none  [on_device(): return (layer_out, new_state, jnp.transpose(new_conv, (2, 0, 1, 3)))]
    slice x1 -> x0, local copies, waits for them, and re-layouts: 0.81 us -> none  [on_device(): new_conv = jnp.concatenate([conv_t[1:], newest[None]], axis=0)]
where the time goes in v3:
time: 55.3 us; the launch traced here: 54.8 us
  Pallas kernels  54.2 us (98%)
  between operations  0.65 us (1%)
    pallas_call x1, Pallas kernels, on_device(): pl.pallas_call(kernel, out_shape=(pltpu.VMEM((32, 128), BF16), pltpu.VMEM...  52.8 us
    pallas_call x1, Pallas kernels, on_device(): pl.pallas_call(write_out, out_shape=tuple((jax.ShapeDtypeStruct(r.shape,...  1.35 us

profile of v3, /device:TPU:1, one launch (start us, length us, event | category | flops | bytes accessed | tf_op | source)
XLA Modules:
  0.0 54.8 jit_solution(12677813637661899021)
XLA Ops:
  0.6 52.8 %shard_map.256 = (bf16[32,128]{1,0:T(8,128)(2,1)S(1)}, f32[32,2,64,128]{3,2,1,0:T(8,128)S(1)}, bf16[3,3,32,128]{3,2,1,0:T(8,128)(2,1)S(1)}) custom-call(bf16[32,2048]{1,0:T(8,128)(2,1)} %residual.1, f32[16,128]{1,0:T(8,128)} %bitcast.16, bf16[128,128]{1,0:T(8,128)(2,1)} %gate_proj.1, bf16[128,128]{1,0:T(8,128)(2,1)} %input_proj.1, ...), custom_call_target="tpu_custom_call" | custom-call | tf_op jit(solution)/shard_map/pallas_call | solution.py:680
  53.5 1.4 %shard_map.257 = (bf16[32,128]{1,0:T(8,128)(2,1)}, f32[32,2,64,128]{3,2,1,0:T(8,128)}, bf16[3,3,32,128]{3,2,1,0:T(8,128)(2,1)}) custom-call(bf16[32,128]{1,0:T(8,128)(2,1)S(1)} %get-tuple-element.9.a, f32[32,2,64,128]{3,2,1,0:T(8,128)S(1)} %get-tuple-element.10.b, bf16[3,3,32,128]{3,2,1,0:T(8,128)(2,1)S(1)} %get-tuple-element.11.c), custom_call_target="tpu_custom_call" | custom-call | tf_op jit(solution)/shard_map/pallas_call | solution.py:737

commit v4 on v3

--- a/solution.py
+++ b/solution.py
@@ -14,6 +14,18 @@
 VM = pl.BlockSpec(memory_space=pltpu.VMEM)
 ANY = pl.BlockSpec(memory_space=pl.ANY)
 HBM = pl.BlockSpec(memory_space=pltpu.HBM)
+
+
+def hops(d):
+    dy, dx = divmod(d, 4)
+    return min(dy, 4 - dy) + min(dx, 4 - dx)
+
+
+FAR = sorted(range(1, 16), key=lambda d: -hops(d))
+NEAR = FAR[::-1]
+FAR_Z = (4, 3, 5, 2, 6, 1, 7)
+NEAR_Z = FAR_Z[::-1]
+FAR_LINE = (2, 1, 3)
 
 
 def dot(a, b, dims=(((1,), (0,)), ((), ()))):
@@ -126,6 +138,10 @@
     rf,
     sr,
     rr,
+    sn,
+    rn,
+    near_sem,
+    far_sem,
 ):
     E = lax.axis_index("ep")
     T = lax.axis_index("tp")
@@ -134,18 +150,28 @@
     pair = Z * 2 + (1 - C)
 
     def ep_at(d):
-        dy, dx = lax.div(d, 4), lax.rem(d, 4)
+        dy, dx = divmod(d, 4)
         return lax.rem(Y + dy, 4) * 4 + lax.rem(X + dx, 4)
 
     def ep_from(d):
-        dy, dx = lax.div(d, 4), lax.rem(d, 4)
+        dy, dx = divmod(d, 4)
         return lax.rem(Y + 4 - dy, 4) * 4 + lax.rem(X + 4 - dx, 4)
+
+    def y_at(d):
+        return lax.rem(Y + d, 4) * 4 + X
+
+    def x_at(d):
+        return Y * 4 + lax.rem(X + d, 4)
 
     def tp_at(d):
         return lax.rem(Z + d, 8) * 2 + C
 
     def loop(lo, hi, fn):
         lax.fori_loop(lo, hi, lambda i, c: (fn(i), c)[1], 0)
+
+    def each(order, fn):
+        for d in order:
+            fn(d)
 
     def send(src, dst, ssem, rsem, ep, tp):
         return pltpu.make_async_remote_copy(
@@ -157,23 +183,6 @@
             device_id_type=MESH,
         )
 
-    bar = pltpu.get_barrier_semaphore()
-    loop(
-        1,
-        16,
-        lambda d: pl.semaphore_signal(
-            bar, inc=1, device_id={"ep": ep_at(d), "tp": T}, device_id_type=MESH
-        ),
-    )
-    loop(
-        1,
-        8,
-        lambda d: pl.semaphore_signal(
-            bar, inc=1, device_id={"ep": E, "tp": tp_at(d)}, device_id_type=MESH
-        ),
-    )
-    pl.semaphore_signal(bar, inc=1, device_id={"ep": E, "tp": pair}, device_id_type=MESH)
-
     chan = pl.ds(pl.multiple_of(T * 128, 128), 128)
     loads = {}
 
@@ -199,6 +208,17 @@
         (write_proj, wq.at[Y, :, pl.ds(0, 128)]),
         (read_proj, wq.at[Y, :, pl.ds(128, 128)]),
     )
+    def signal(sem, ep, tp):
+        pl.semaphore_signal(
+            sem, inc=1, device_id={"ep": ep, "tp": tp}, device_id_type=MESH
+        )
+
+    bar = pltpu.get_barrier_semaphore()
+    each(FAR_LINE, lambda d: signal(bar, x_at(d), T))
+    each(FAR_LINE, lambda d: signal(bar, y_at(d), T))
+    each((1, 7), lambda d: signal(bar, E, tp_at(d)))
+    signal(bar, E, pair)
+
     load(
         "small",
         (step_proj, sproj),
@@ -232,19 +252,15 @@
     for t in range(16):
         blk = (rv[:, lanes(t)] * scale * mgain[t : t + 1, :]).astype(BF16)
         nat[:, lanes(t)] = blk
-        np_[t // 4, :, lanes(t % 4)] = blk
-        nq[t % 4, :, lanes(t // 4)] = blk
-    rp[0] = np_[Y]
-    rq[0] = nq[X]
+        np_[t // 4, t % 4 // 2, :, lanes(t % 2)] = blk
+        nq[t % 4, t // 8, :, lanes(t // 4 % 2)] = blk
+    for h in range(2):
+        rp[h, 0] = np_[Y, h]
+        rq[h, 0] = nq[X, h]
 
     loaded("proj")
-    pl.semaphore_wait(bar, 23)
-
-    def y_at(d):
-        return lax.rem(Y + d, 4) * 4 + X
-
-    def x_at(d):
-        return Y * 4 + lax.rem(X + d, 4)
+    pl.semaphore_wait(bar, 9)
+    each((1, 7), lambda d: signal(near_sem, E, tp_at(d)))
 
     def w_p(d):
         return send(wp.at[X], wp.at[X], s1.at[d - 1], r1.at[d - 1], x_at(d), T)
@@ -254,16 +270,16 @@
 
     def n_p(d):
         return send(
-            np_.at[lax.rem(Y + d, 4)], rp.at[d], s1.at[d + 5], r1.at[d + 5], y_at(d), T
+            np_.at[lax.rem(Y + d, 4), C], rp.at[C, d], s1.at[d + 5], r1.at[d + 5], y_at(d), T
         )
 
     def n_q(d):
         return send(
-            nq.at[lax.rem(X + d, 4)], rq.at[d], s1.at[d + 8], r1.at[d + 8], x_at(d), T
-        )
-
-    for f in (w_p, w_q, n_p, n_q):
-        loop(1, 4, lambda d, f=f: f(d).start())
+            nq.at[lax.rem(X + d, 4), C], rq.at[C, d], s1.at[d + 8], r1.at[d + 8], x_at(d), T
+        )
+
+    for f in (n_p, n_q, w_p, w_q):
+        each(FAR_LINE, lambda d, f=f: f(d).start())
 
     loaded("small")
     raw = dot(nat[...], sproj[...], (((1,), (1,)), ((), ())))
@@ -306,6 +322,8 @@
     place[1] = spots[0] * rw[0:1, :] + spots[1] * rw[1:2, :]
 
     loaded("state")
+    pl.semaphore_wait(near_sem, 2)
+    each((2, 6), lambda d: signal(far_sem, E, tp_at(d)))
 
     def split(s):
         v = st[s].reshape(128, 128)
@@ -318,9 +336,29 @@
         for c in range(3):
             new_conv[k, c] = cst[k + 1, c]
 
-    loop(1, 4, lambda d: w_p(d).wait_recv())
-    loop(1, 4, lambda d: n_p(d).wait_recv())
-    part_p = dot(rp[...].reshape(128, 512), wp[...].reshape(512, 256))
+    def pass_p(side):
+        return send(
+            rp.at[side, pl.ds(1, 3)], rp.at[side, pl.ds(1, 3)], sn.at[0], rn.at[0], E, pair
+        )
+
+    def pass_q(side):
+        return send(
+            rq.at[side, pl.ds(1, 3)], rq.at[side, pl.ds(1, 3)], sn.at[1], rn.at[1], E, pair
+        )
+
+    each((1, 3, 2), lambda d: n_p(d).wait_recv())
+    pass_p(C).start()
+    each((1, 3, 2), lambda d: n_q(d).wait_recv())
+    pass_q(C).start()
+    pass_p(1 - C).wait_recv()
+    each((1, 3, 2), lambda d: w_p(d).wait_recv())
+
+    def projected(rows, weights):
+        return dot(rows[0].reshape(128, 256), weights[0:2].reshape(256, 256)) + dot(
+            rows[1].reshape(128, 256), weights[2:4].reshape(256, 256)
+        )
+
+    part_p = projected(rp, wp)
     sp[...] = part_p.astype(BF16).reshape(4, 32, 256)
 
     def back_p(d):
@@ -328,10 +366,10 @@
             sp.at[d], r2p.at[d - 1], s2.at[d - 1], r2.at[d - 1], y_at(4 - d), T
         )
 
-    loop(1, 4, lambda d: back_p(d).start())
-    loop(1, 4, lambda d: w_q(d).wait_recv())
-    loop(1, 4, lambda d: n_q(d).wait_recv())
-    part_q = dot(rq[...].reshape(128, 512), wq[...].reshape(512, 256))
+    each(FAR_LINE, lambda d: back_p(d).start())
+    pass_q(1 - C).wait_recv()
+    each((1, 3, 2), lambda d: w_q(d).wait_recv())
+    part_q = projected(rq, wq)
     sq[...] = part_q.astype(BF16).reshape(4, 32, 256)
 
     def back_q(d):
@@ -339,13 +377,14 @@
             sq.at[d], r2q.at[d - 1], s2.at[d + 2], r2.at[d + 2], x_at(4 - d), T
         )
 
-    loop(1, 4, lambda d: back_q(d).start())
+    each(FAR_LINE, lambda d: back_q(d).start())
+    pl.semaphore_wait(far_sem, 2)
     own_p, own_q = part_p[0:32], part_q[0:32]
     loaded("op")
-    loop(1, 4, lambda d: back_p(d).wait_recv())
+    each((1, 3, 2), lambda d: back_p(d).wait_recv())
     for d in range(3):
         own_p = own_p + r2p[d].astype(F32)
-    loop(1, 4, lambda d: back_q(d).wait_recv())
+    each((1, 3, 2), lambda d: back_q(d).wait_recv())
     for d in range(3):
         own_q = own_q + r2q[d].astype(F32)
     z_proj = own_p[:, 0:128].astype(BF16).astype(F32)
@@ -419,11 +458,11 @@
             rs_out.at[z_block(d)], rs_in.at[d - 1], sz.at[d - 1], rz.at[d - 1], E, tp_at(d)
         )
 
-    loop(1, 8, lambda d: scatter(d).start())
+    each(FAR_Z, lambda d: scatter(d).start())
     total = mixer_own[Z]
     loop(0, 2, tokens)
     resid_cols = res[:, chan].astype(F32)
-    loop(1, 8, lambda d: scatter(d).wait_recv())
+    each(NEAR_Z, lambda d: scatter(d).wait_recv())
     for d in range(7):
         total = total + rs_in[d].astype(F32)
     rm[C, Z] = (resid_cols + total).astype(BF16)
@@ -438,10 +477,10 @@
             rm.at[C, z_block(8 - d)], rm.at[C, z_block(8 - d)], sz.at[d + 6], rz.at[d + 6], E, tp_at(d)
         )
 
-    loop(1, 8, lambda d: gather(d).start())
+    each(FAR_Z, lambda d: gather(d).start())
     loop(2, 4, tokens)
     loaded("dense", "experts", "ffn")
-    loop(1, 8, lambda d: gather_in(d).wait_recv())
+    each(NEAR_Z, lambda d: gather_in(d).wait_recv())
     swap_resid = to_pair(rm.at[C], rm.at[C], 1)
     swap_resid.start()
 
@@ -460,7 +499,7 @@
     def forward_in(d):
         return send(rx.at[1 - C, d], rx.at[1 - C, d], sf.at[d], rf.at[d], E, pair)
 
-    loop(1, 16, lambda d: dispatch(d).start())
+    each(FAR, lambda d: dispatch(d).start())
     forward(0).start()
 
     to_pair(rm.at[1 - C], rm.at[1 - C], 1).wait_recv()
@@ -490,8 +529,8 @@
         dispatch(d).wait_recv()
         forward(d).start()
 
-    loop(1, 16, arrive)
-    loop(0, 16, lambda d: forward_in(d).wait_recv())
+    each(NEAR, arrive)
+    each([0] + NEAR, lambda d: forward_in(d).wait_recv())
 
     def side(c):
         v = rx[c].astype(F32).reshape(16, 2, 8, 512)
@@ -514,43 +553,56 @@
         hid = silu(hid[:, 0:128]) * hid[:, 128:256]
         mine = (row % 8 >= 4) if j else (row % 8 < 4)
         hids.append(jnp.where(mine, hid, 0.0).astype(BF16))
-    part = dot(jnp.concatenate(hids, axis=1), dn[...].reshape(256, 2048))
-
-    def folded(v):
-        lo = v[0].reshape(16, 8, 512)
-        hi = v[1].reshape(16, 8, 512)
-        return jnp.concatenate([lo, hi], axis=1)
+    hid = jnp.concatenate(hids, axis=1)
+
+    def swap_expert(q):
+        return to_pair(half_e.at[1 - C, q], pair_e.at[q], 3 + q)
 
     for q in range(2):
-        even = jnp.concatenate([part[:, lanes(2 * z)] for z in range(4 * q, 4 * q + 4)], axis=1)
-        odd = jnp.concatenate([part[:, lanes(2 * z + 1)] for z in range(4 * q, 4 * q + 4)], axis=1)
+        part = dot(hid, dn[:, :, q * 1024 : (q + 1) * 1024].reshape(256, 1024))
+        even = jnp.concatenate([part[:, lanes(2 * z)] for z in range(4)], axis=1)
+        odd = jnp.concatenate([part[:, lanes(2 * z + 1)] for z in range(4)], axis=1)
         half_e[0, q] = even.astype(BF16)
         half_e[1, q] = odd.astype(BF16)
         own_e[q] = jnp.where(C == 0, even, odd)
-    swap_expert = to_pair(half_e.at[1 - C], pair_e, 3)
-    swap_expert.start()
-    swap_expert.wait_recv()
-    both = own_e[...] + pair_e[...].astype(F32)
-    ret[...] = folded(both).astype(BF16)
-    back[E] = ret[0]
-
-    def give_back(d):
-        return send(ret.at[d], back.at[E], sr.at[d - 1], rr.at[d - 1], ep_from(d), T)
-
-    def give_back_in(d):
-        return send(ret.at[d], back.at[ep_at(d)], sr.at[d - 1], rr.at[d - 1], ep_from(d), T)
-
-    loop(1, 16, lambda d: give_back(d).start())
+        swap_expert(q).start()
+
+    def give_back(d, q):
+        i = q * 15 + d - 1
+        return send(ret.at[q, d], back.at[q, E], sr.at[i], rr.at[i], ep_from(d), T)
+
+    def give_back_in(d, q):
+        i = q * 15 + d - 1
+        return send(ret.at[q, d], back.at[q, ep_at(d)], sr.at[i], rr.at[i], ep_from(d), T)
+
+    for q in range(2):
+        swap_expert(q).wait_recv()
+        both = own_e[q] + pair_e[q].astype(F32)
+        lo, hi = both[:, :256].reshape(16, 8, 256), both[:, 256:].reshape(16, 8, 256)
+        ret[q] = jnp.concatenate([lo, hi], axis=1).astype(BF16)
+        back[q, E] = ret[q, 0]
+        each(FAR, lambda d, q=q: give_back(d, q).start())
+
     swap_dense.wait_recv()
     own_d[...] = own_d[...] + pair_d[...].astype(F32)
     weight = place[1]
     w_hi = weight.astype(BF16)
     w_lo = (weight - w_hi.astype(F32)).astype(BF16)
-    loop(1, 16, lambda d: give_back_in(d).wait_recv())
-    v = back[...].astype(F32).reshape(16, 2, 8, 512)
+    for f in (w_p, w_q, n_p, n_q, back_p, back_q):
+        loop(1, 4, lambda d, f=f: f(d).wait_send())
+    for f in (scatter, gather):
+        loop(1, 8, lambda d, f=f: f(d).wait_send())
+    each(FAR, lambda d: dispatch(d).wait_send())
+    loop(0, 16, lambda d: forward(d).wait_send())
+    for c in (pass_p(C), pass_q(C), swap_mixer, swap_resid, swap_dense):
+        c.wait_send()
+    each(range(2), lambda q: swap_expert(q).wait_send())
     first = (((0,), (0,)), ((), ()))
     for q in range(2):
-        rows = v[:, q].reshape(128, 512).astype(BF16)
+        each(NEAR, lambda d, q=q: give_back_in(d, q).wait_recv())
+        v = back[q].astype(F32).reshape(16, 2, 8, 256)
+        rows = jnp.concatenate([v[:, i].reshape(128, 256) for i in range(2)], axis=1)
+        rows = rows.astype(BF16)
         mix = dot(w_hi, rows, first) + dot(w_lo, rows, first)
         for z in range(4):
             own_d[4 * q + z] = own_d[4 * q + z] + mix[:, lanes(z)]
@@ -561,22 +613,16 @@
             rs2_out.at[z_block(d)], rs2_in.at[d - 1], sz.at[d + 13], rz.at[d + 13], E, tp_at(d)
         )
 
-    loop(1, 8, lambda d: scatter2(d).start())
+    each(FAR_Z, lambda d: scatter2(d).start())
     total = own_d[Z] + rm[C, Z].astype(F32)
-    loop(1, 8, lambda d: scatter2(d).wait_recv())
+    each(NEAR_Z, lambda d: scatter2(d).wait_recv())
     for d in range(7):
         total = total + rs2_in[d].astype(F32)
     layer_out[...] = total.astype(BF16)
 
-    for f in (w_p, w_q, n_p, n_q, back_p, back_q):
-        loop(1, 4, lambda d, f=f: f(d).wait_send())
-    for f in (scatter, gather, scatter2):
-        loop(1, 8, lambda d, f=f: f(d).wait_send())
-    for f in (dispatch, give_back):
-        loop(1, 16, lambda d, f=f: f(d).wait_send())
-    loop(0, 16, lambda d: forward(d).wait_send())
-    for s in (swap_mixer, swap_resid, swap_dense, swap_expert):
-        s.wait_send()
+    for q in range(2):
+        each(FAR, lambda d, q=q: give_back(d, q).wait_send())
+    loop(1, 8, lambda d: scatter2(d).wait_send())
 
 
 def write_out(a, b, c, a_out, b_out, c_out, sem):
@@ -613,10 +659,10 @@
     ((2048, 256), BF16),
     ((128, 2048), BF16),
     ((32, 2048), BF16),
-    ((4, 32, 512), BF16),
-    ((4, 32, 512), BF16),
-    ((4, 32, 512), BF16),
-    ((4, 32, 512), BF16),
+    ((4, 2, 32, 256), BF16),
+    ((4, 2, 32, 256), BF16),
+    ((2, 4, 32, 256), BF16),
+    ((2, 4, 32, 256), BF16),
     ((4, 32, 256), BF16),
     ((4, 32, 256), BF16),
     ((3, 32, 256), BF16),
@@ -637,8 +683,8 @@
     ((2, 2, 128, 512), BF16),
     ((2, 128, 512), F32),
     ((2, 128, 512), BF16),
-    ((16, 16, 512), BF16),
-    ((16, 16, 512), BF16),
+    ((2, 16, 16, 256), BF16),
+    ((2, 16, 16, 256), BF16),
     ((32, 2048), BF16),
     ((2, 8, 32, 128), BF16),
     ((8, 32, 128), F32),
@@ -695,14 +741,18 @@
             pltpu.SemaphoreType.DMA((6,)),
             pltpu.SemaphoreType.DMA((21,)),
             pltpu.SemaphoreType.DMA((21,)),
-            pltpu.SemaphoreType.DMA((4,)),
-            pltpu.SemaphoreType.DMA((4,)),
+            pltpu.SemaphoreType.DMA((5,)),
+            pltpu.SemaphoreType.DMA((5,)),
             pltpu.SemaphoreType.DMA((15,)),
             pltpu.SemaphoreType.DMA((15,)),
             pltpu.SemaphoreType.DMA((16,)),
             pltpu.SemaphoreType.DMA((16,)),
-            pltpu.SemaphoreType.DMA((15,)),
-            pltpu.SemaphoreType.DMA((15,)),
+            pltpu.SemaphoreType.DMA((30,)),
+            pltpu.SemaphoreType.DMA((30,)),
+            pltpu.SemaphoreType.DMA((2,)),
+            pltpu.SemaphoreType.DMA((2,)),
+            pltpu.SemaphoreType.REGULAR,
+            pltpu.SemaphoreType.REGULAR,
         ],
         compiler_params=pltpu.CompilerParams(
             collective_id=0, has_side_effects=True, vmem_limit_bytes=64_400_000

time: 55.3 us -> 51.3 us (0.928)
  Pallas kernels: 54.2 us -> 50.1 us
    pallas_call x1, Pallas kernels: 52.8 us -> 48.8 us  [on_device(): pl.pallas_call(kernel, out_shape=(pltpu.VMEM((32, 128), BF16), pltpu.VMEM...]
where the time goes in v4:
time: 51.3 us; the launch traced here: 50.8 us
  Pallas kernels  50.1 us (98%)
  between operations  0.65 us (1%)
    pallas_call x1, Pallas kernels, on_device(): pl.pallas_call(kernel, out_shape=(pltpu.VMEM((32, 128), BF16), pltpu.VMEM...  48.8 us
    pallas_call x1, Pallas kernels, on_device(): pl.pallas_call(write_out, out_shape=tuple((jax.ShapeDtypeStruct(r.shape,...  1.35 us

profile of v4, /device:TPU:1, one launch (start us, length us, event | category | flops | bytes accessed | tf_op | source)
XLA Modules:
  0.0 50.8 jit_solution(3511196145250026640)
XLA Ops:
  0.6 48.8 %shard_map.256 = (bf16[32,128]{1,0:T(8,128)(2,1)S(1)}, f32[32,2,64,128]{3,2,1,0:T(8,128)S(1)}, bf16[3,3,32,128]{3,2,1,0:T(8,128)(2,1)S(1)}) custom-call(bf16[32,2048]{1,0:T(8,128)(2,1)} %residual.1, f32[16,128]{1,0:T(8,128)} %bitcast.16, bf16[128,128]{1,0:T(8,128)(2,1)} %gate_proj.1, bf16[128,128]{1,0:T(8,128)(2,1)} %input_proj.1, ...), custom_call_target="tpu_custom_call" | custom-call | tf_op jit(solution)/shard_map/pallas_call | solution.py:726
  49.4 1.4 %shard_map.257 = (bf16[32,128]{1,0:T(8,128)(2,1)}, f32[32,2,64,128]{3,2,1,0:T(8,128)}, bf16[3,3,32,128]{3,2,1,0:T(8,128)(2,1)}) custom-call(bf16[32,128]{1,0:T(8,128)(2,1)S(1)} %get-tuple-element.9.a, f32[32,2,64,128]{3,2,1,0:T(8,128)S(1)} %get-tuple-element.10.b, bf16[3,3,32,128]{3,2,1,0:T(8,128)(2,1)S(1)} %get-tuple-element.11.c), custom_call_target="tpu_custom_call" | custom-call | tf_op jit(solution)/shard_map/pallas_call | solution.py:787
